TPU v7x, 32 devices: a whole 2x2x4 slice. The times are simulated.
32 devices in a mesh: ep: 16 (over z, y, x), tp: 2 (over core).
Axes of the slice: x: 2, y: 2, z: 4, core: 2. Of those that a mesh axis runs over, the one named last changes fastest.
Arguments:
- tokens: bfloat16 [256, 2048], P('ep'), may hold values from -6 to 6
- lengths: int32 [256], P('ep'), may hold values from 1 to 1024, as said below
- attn_gain: float32 [2048], replicated, may hold values from 0.1 to 1.9
- w_query: bfloat16 [2048, 1024], P(None, 'tp'), may hold values from -0.125 to 0.125
- w_key: bfloat16 [2048, 128], P(None, 'tp'), may hold values from -0.125 to 0.125
- w_value: bfloat16 [2048, 128], P(None, 'tp'), may hold values from -0.125 to 0.125
- head_bias: float32 [16], P('tp'), may hold values from -7 to -2
- key_cache: bfloat16 [256, 2, 64, 1024], P('ep', 'tp'), may hold values from -6 to 6
- value_cache: bfloat16 [256, 2, 64, 1024], P('ep', 'tp'), may hold values from -6 to 6
- w_attn_out: bfloat16 [1024, 2048], P('tp'), may hold values from -0.1875 to 0.1875
- ffn_gain: float32 [2048], replicated, may hold values from 0.1 to 1.9
- w_router: bfloat16 [2048, 16], replicated, may hold values from -0.125 to 0.125
- routes: int32 [256, 6], P('ep'), may hold values from 0 to 15, all different within a row; in each aligned block of 16 rows (0 to 15, 16 to 31, ...) at most 12 rows name the same one
- w_dense_gate: bfloat16 [2048, 512], P('ep', 'tp'), may hold values from -0.125 to 0.125
- w_dense_up: bfloat16 [2048, 512], P('ep', 'tp'), may hold values from -0.125 to 0.125
- w_dense_down: bfloat16 [512, 2048], P('tp', 'ep'), may hold values from -0.25 to 0.25
- dense_mix: float32 [2048], replicated, may hold values from -0.125 to 0.125
- w_expert_gate: bfloat16 [16, 2048, 512], P('ep', None, 'tp'), may hold values from -0.125 to 0.125
- w_expert_up: bfloat16 [16, 2048, 512], P('ep', None, 'tp'), may hold values from -0.125 to 0.125
- w_expert_down: bfloat16 [16, 512, 2048], P('ep', 'tp'), may hold values from -0.25 to 0.25
Outputs:
- layer_out: bfloat16 [256, 2048], P('ep', 'tp')
- new_keys: bfloat16 [256, 128], P('ep', 'tp')
- new_values: bfloat16 [256, 128], P('ep', 'tp')
Inputs may be any that keep to these rules, and one draw needn't show every extreme that they name: `lengths`: every sequence holds between 1 and 1024 cached positions; in every draw some sequence holds exactly 1024. `routes`: each token names 6 different experts. Among the rows of one device no expert is named by more than 12 rows.
All inputs are finite; a program needn't handle non-finite values.
Results may differ from a plain program's by a relative error of at most 0.014.
Values may be sent and summed in bfloat16 or wider, within the bound.
A program may use at most 64 MiB of HBM per device.

v0:
```python
import jax
import jax.numpy as jnp
from jax import lax
from jax.sharding import PartitionSpec as P


def rms_scale(values, gain):
    wide = values.astype(jnp.float32)
    return wide * lax.rsqrt(jnp.mean(wide * wide, axis=-1, keepdims=True) + 1e-06) * gain


def stick_read(queries, lengths, head_bias, key_cache, value_cache):
    seq_count, local_kv, head_dim, cache_len = key_cache.shape
    group_size = head_bias.shape[0] // local_kv
    grouped = queries.reshape(seq_count, local_kv, group_size, head_dim)
    head_shift = head_bias.reshape(1, local_kv, group_size, 1)
    span_len = min(512, cache_len)
    block_count = (jnp.max(lengths) + span_len - 1) // span_len
    span_index = lax.iota(jnp.int32, span_len)
    after_mask = (span_index[:, None] > span_index[None, :]).astype(jnp.float32)

    def visit(visit_index, carry):
        totals, log_later = carry
        first = (block_count - 1 - visit_index) * span_len
        key_block = lax.dynamic_slice_in_dim(key_cache, first, span_len, 3)
        value_block = lax.dynamic_slice_in_dim(value_cache, first, span_len, 3)
        scores = (
            jnp.einsum("skgd,skdc->skgc", grouped, key_block, preferred_element_type=jnp.float32)
            * head_dim ** (-0.5)
            + head_shift
        )
        positions = first + span_index
        visible = (positions[None, :] < lengths[:, None])[:, None, None, :]
        log_keep = jnp.where(visible, jax.nn.log_sigmoid(-scores), 0.0)
        log_after = (
            jnp.einsum("skgj,jc->skgc", log_keep, after_mask, precision=lax.Precision.HIGHEST)
            + log_later[..., None]
        )
        weights = jnp.where(visible, jnp.exp(jax.nn.log_sigmoid(scores) + log_after), 0.0).astype(
            jnp.bfloat16
        )
        totals = totals + jnp.einsum(
            "skgc,skdc->skgd", weights, value_block, preferred_element_type=jnp.float32
        )
        return (totals, log_later + jnp.sum(log_keep, axis=3))

    start_totals = jnp.zeros((seq_count, local_kv, group_size, head_dim), jnp.float32)
    start_later = jnp.zeros((seq_count, local_kv, group_size), jnp.float32)
    totals, unused_later = lax.fori_loop(0, block_count, visit, (start_totals, start_later))
    return totals.reshape(seq_count, -1).astype(jnp.bfloat16)


def expert_math(inputs, w_expert_gate, w_expert_up, w_expert_down):
    gate_rows = jnp.einsum(
        "njcd,jdf->njcf", inputs, w_expert_gate, preferred_element_type=jnp.float32
    )
    up_rows = jnp.einsum("njcd,jdf->njcf", inputs, w_expert_up, preferred_element_type=jnp.float32)
    hidden = (jax.nn.silu(gate_rows) * up_rows).astype(jnp.bfloat16)
    partial_value = jnp.einsum(
        "njcf,jfd->njcd", hidden, w_expert_down, preferred_element_type=jnp.float32
    ).astype(jnp.bfloat16)
    return (
        lax.psum_scatter(partial_value, "tp", scatter_dimension=3, tiled=True)
        .astype(jnp.float32)
        .astype(jnp.bfloat16)
    )


def shards(
    tokens,
    lengths,
    attn_gain,
    w_query,
    w_key,
    w_value,
    head_bias,
    key_cache,
    value_cache,
    w_attn_out,
    ffn_gain,
    w_router,
    routes,
    w_dense_gate,
    w_dense_up,
    w_dense_down,
    dense_mix,
    w_expert_gate,
    w_expert_up,
    w_expert_down,
):
    seq_count, model_width = tokens.shape
    normed = rms_scale(tokens, attn_gain).astype(jnp.bfloat16)
    new_keys = jnp.dot(normed, w_key, preferred_element_type=jnp.float32).astype(jnp.bfloat16)
    new_values = jnp.dot(normed, w_value, preferred_element_type=jnp.float32).astype(jnp.bfloat16)
    queries = jnp.dot(normed, w_query, preferred_element_type=jnp.float32).astype(jnp.bfloat16)
    heads_out = stick_read(queries, lengths, head_bias, key_cache, value_cache)
    attn_partial = jnp.dot(heads_out, w_attn_out, preferred_element_type=jnp.float32).astype(
        jnp.bfloat16
    )
    attn = lax.psum(attn_partial, "tp").astype(jnp.float32)
    residual = (tokens.astype(jnp.float32) + attn).astype(jnp.bfloat16)
    normed2 = rms_scale(residual, ffn_gain).astype(jnp.bfloat16)
    expert_total = w_router.shape[1]
    top_count = routes.shape[1]
    probs = jax.nn.sigmoid(jnp.dot(normed2, w_router, preferred_element_type=jnp.float32))
    hits = routes[:, :, None] == lax.iota(jnp.int32, expert_total)[None, None, :]
    picked = jnp.sum(jnp.where(hits, probs[:, None, :], 0.0), axis=-1)
    gates = picked / jnp.sum(picked, axis=-1, keepdims=True) * 2.5
    capacity = max(2, 2 * seq_count * top_count // expert_total)
    slot_total = expert_total * capacity
    flat_routes = routes.reshape(-1)
    route_count = flat_routes.shape[0]
    matching = flat_routes[:, None] == flat_routes[None, :]
    earlier = lax.iota(jnp.int32, route_count)[:, None] > lax.iota(jnp.int32, route_count)[None, :]
    slot_rank = jnp.sum(jnp.logical_and(matching, earlier).astype(jnp.int32), axis=1)
    target = flat_routes * capacity + slot_rank
    one_hot = (target[:, None] == lax.iota(jnp.int32, slot_total)[None, :]).astype(jnp.bfloat16)
    dispatch = jnp.sum(one_hot.reshape(seq_count, top_count, slot_total), axis=1)
    send_rows = jnp.einsum(
        "sr,sd->rd", dispatch, normed2, preferred_element_type=jnp.float32
    ).astype(jnp.bfloat16)
    send_rows = send_rows.reshape(expert_total, capacity, model_width)
    local_experts = w_expert_gate.shape[0]
    received = lax.all_to_all(send_rows, "ep", split_axis=0, concat_axis=0, tiled=True)
    source_count = received.shape[0] // local_experts
    item_count = received.shape[1]
    inputs = received.reshape(source_count, local_experts, item_count, model_width)
    summed = expert_math(inputs, w_expert_gate, w_expert_up, w_expert_down)
    summed = summed.reshape(source_count * local_experts, item_count, summed.shape[3])
    returned = lax.all_to_all(summed, "ep", split_axis=0, concat_axis=0, tiled=True)
    half_width = returned.shape[2]
    route_rows = returned.reshape(slot_total, half_width)[target]
    route_rows = route_rows.reshape(seq_count, top_count, half_width)
    routed = jnp.sum(gates[:, :, None] * route_rows.astype(jnp.float32), axis=1)
    features2 = lax.all_to_all(normed2, "ep", split_axis=1, concat_axis=0, tiled=True)
    paired_weights = jnp.concatenate([w_dense_gate, w_dense_up], axis=1)
    paired = lax.psum_scatter(
        jnp.dot(features2, paired_weights, preferred_element_type=jnp.float32),
        "ep",
        scatter_dimension=0,
        tiled=True,
    )
    hidden_cols = w_dense_gate.shape[1]
    dense_gate_rows = paired[:, :hidden_cols]
    dense_up_rows = paired[:, hidden_cols:]
    dense_hidden = (jax.nn.silu(dense_gate_rows) * dense_up_rows).astype(jnp.bfloat16)
    dense_columns = jnp.dot(
        lax.all_gather(dense_hidden, "ep", axis=0, tiled=True),
        w_dense_down,
        preferred_element_type=jnp.float32,
    )
    dense_partial = lax.all_to_all(
        dense_columns.astype(jnp.bfloat16), "ep", split_axis=0, concat_axis=1, tiled=True
    )
    dense = lax.psum_scatter(dense_partial, "tp", scatter_dimension=1, tiled=True).astype(
        jnp.float32
    )
    mix_gate = jax.nn.sigmoid(jnp.sum(normed2.astype(jnp.float32) * dense_mix, axis=-1))
    offset = lax.axis_index("tp") * half_width
    residual_half = lax.dynamic_slice_in_dim(residual, offset, half_width, 1)
    layer_out = (residual_half.astype(jnp.float32) + mix_gate[:, None] * dense + routed).astype(
        jnp.bfloat16
    )
    return (layer_out, new_keys, new_values)


def solution(mesh):
    return jax.shard_map(
        shards,
        mesh=mesh,
        in_specs=(
            P("ep", None),
            P("ep"),
            P(),
            P(None, "tp"),
            P(None, "tp"),
            P(None, "tp"),
            P("tp"),
            P("ep", "tp", None, None),
            P("ep", "tp", None, None),
            P("tp", None),
            P(),
            P(),
            P("ep", None),
            P("ep", "tp"),
            P("ep", "tp"),
            P("tp", "ep"),
            P(),
            P("ep", None, "tp"),
            P("ep", None, "tp"),
            P("ep", "tp", None),
        ),
        out_specs=(P("ep", "tp"), P("ep", "tp"), P("ep", "tp")),
        check_vma=False,
    )
```

profile of v0, /device:TPU:7, one launch (start us, length us, event | category | flops | bytes accessed | tf_op | source)
XLA Modules:
  0.0 214.8 jit_solution(16179048854171437925)
XLA Ops:
  7.2 1.4 reduce_max.9
  10.3 2.1 convolution_convert_fusion.4
  12.5 7.7 %while.15 = (s32[]{:T(128)}, f32[16,1,8,64]{3,2,0,1:T(8,128)S(1)}, f32[16,1,8]{0,2,1:T(8,128)S(1)}, s32[]{:T(128)}, s32[]{:T(128)}, /*index=5*/s32[16]{0:T(128)S...) while((s32[]{:T(128)}, f32[16,1,8,64]{3,2,0,1:T(8,128)S(1)}, ...), condition=%wide.region_4.5_spmd.clone, body=%wide.region_2.4_spmd.clone.sunk | while | flops 422003200 | bytes 11420487 | solution.py:49
  12.7 1.6 fusion.88
  16.5 1.7 fusion.88
  20.4 1.0 convolution_convert_fusion.2
  22.1 18.2 %all-reduce.2.cloned.1.call-done = bf16[16,2048]{1,0:T(8,128)(2,1)} async-done(((bf16[16,2048]{1,0:T(8,128)(2,1)}), bf16[16,2048]{1,0:T(8,128)(2,1)}) %all-reduce.2.cloned.1.call-update) | async-done | bytes 65552 | tf_op jit(solution)/shard_map/psum | solution.py:100
  42.2 6.4 %all-to-all-start = ((bf16[16,16,128]{2,0,1:T(8,128)(2,1)}), bf16[16,16,128]{2,0,1:T(8,128)(2,1)S(1)}, u32[]{:S(2)}, u32[]{:S(2)}) async-start(bf16[16,16,128]{2,0,1:T(8,128)(2,1)} %bitcast.105), calls=%async_computation | async-start | bytes 131072 | tf_op jit(solution)/shard_map/all_to_all | solution.py:135
  49.0 1.2 reshape.240
  50.2 2.9 %all-to-all-done = bf16[16,16,128]{2,0,1:T(8,128)(2,1)S(1)} async-done(((bf16[16,16,128]{2,0,1:T(8,128)(2,1)}), bf16[16,16,128]{2,0,1:T(8,128)(2,1)S(1)}, u32[]{:S(2)}, u32[]{:S(2)}) %all-to-all-start) | async-done | bytes 65568 | tf_op jit(solution)/shard_map/all_to_all | solution.py:135
  53.1 5.4 %all-to-all-start.2 = ((bf16[16,12,2048]{2,1,0:T(8,128)(2,1)}), bf16[16,12,2048]{2,1,0:T(8,128)(2,1)S(1)}, u32[]{:S(2)}, u32[]{:S(2)}) async-start(bf16[16,12,2048]{2,1,0:T(8,128)(2,1)} %reshape.240), calls=%async_computation.4 | async-start | bytes 2097152 | tf_op jit(solution)/shard_map/all_to_all | solution.py:124
  58.6 1.0 fusion.44
  59.8 21.6 %all-to-all-done.2 = bf16[16,12,2048]{2,1,0:T(8,128)(2,1)S(1)} async-done(((bf16[16,12,2048]{2,1,0:T(8,128)(2,1)}), bf16[16,12,2048]{2,1,0:T(8,128)(2,1)S(1)}, u32[]{:S(2)}, u32[]{:S(2)}) %all-to-all-start.2) | async-done | bytes 786464 | tf_op jit(solution)/shard_map/all_to_all | solution.py:124
  81.4 1.8 convolution_bitcast_fusion.2
  84.4 1.3 fusion.27
  87.4 34.8 %reduce-scatter.4.cloned.1.call-done = f32[16,512]{1,0:T(8,128)} async-done(((f32[256,512]{1,0:T(8,128)}), f32[16,512]{1,0:T(8,128)}) %reduce-scatter.4.cloned.1.call-update) | async-done | bytes 32784 | tf_op jit(solution)/shard_map/reduce_scatter | solution.py:137
  123.0 34.0 %all_gather.3 = bf16[256,256]{1,0:T(8,128)(2,1)S(1)} all-gather(bf16[16,256]{1,0:T(8,128)(2,1)S(1)} %fusion.52), channel_id=1, replica_groups=mesh['ep'=16,'tp'=2] {'ep'}, dimensions={0}, use_global_device_ids=true | all-gather | bytes 139264 | tf_op jit(solution)/shard_map/all_gather | solution.py:148
  157.8 7.4 %all-to-all-start.1 = ((bf16[16,16,128]{2,1,0:T(8,128)(2,1)}), bf16[16,16,128]{2,1,0:T(8,128)(2,1)S(1)}, u32[]{:S(2)}, u32[]{:S(2)}) async-start(bf16[16,16,128]{2,1,0:T(8,128)(2,1)} %bitcast.5), calls=%async_computation.2 | async-start | bytes 131072 | tf_op jit(solution)/shard_map/all_to_all | solution.py:152
  165.7 2.0 copy.64
  167.7 2.1 all-to-all-done.1
  169.8 5.4 %all-to-all-start.3 = ((bf16[16,12,1024]{2,1,0:T(8,128)(2,1)}), bf16[16,12,1024]{2,1,0:T(8,128)(2,1)S(1)}, u32[]{:S(2)}, u32[]{:S(2)}) async-start(bf16[16,12,1024]{2,1,0:T(8,128)(2,1)} %copy.64), calls=%async_computation.6 | async-start | bytes 1048576 | tf_op jit(solution)/shard_map/all_to_all | solution.py:130
  175.9 7.4 %all-to-all-done.3 = bf16[16,12,1024]{2,1,0:T(8,128)(2,1)S(1)} async-done(((bf16[16,12,1024]{2,1,0:T(8,128)(2,1)}), bf16[16,12,1024]{2,1,0:T(8,128)(2,1)S(1)}, u32[]{:S(2)}, u32[]{:S(2)}) %all-to-all-start.3) | async-done | bytes 393248 | tf_op jit(solution)/shard_map/all_to_all | solution.py:130
  184.5 22.4 %reduce-scatter.6.cloned.1.call-done = bf16[16,1024]{1,0:T(8,128)(2,1)} async-done(((bf16[16,2048]{1,0:T(8,128)(2,1)}), bf16[16,1024]{1,0:T(8,128)(2,1)}) %reduce-scatter.6.cloned.1.call-update) | async-done | bytes 32784 | tf_op jit(solution)/shard_map/reduce_scatter | solution.py:155
  206.9 1.4 add_convert_fusion
  (96 shorter events, 15.6 us)
Async XLA Ops:
  7.2 13.3 %copy-start = (bf16[512,2048]{1,0:T(8,128)(2,1)S(1)}, bf16[512,2048]{1,0:T(8,128)(2,1)}, u32[]{:S(2)}) copy-start(bf16[512,2048]{1,0:T(8,128)(2,1)} %param.31) | copy-start | bytes 6291460
  7.2 5.3 %copy-start.9 = (s32[16]{0:T(128)S(1)}, s32[16]{0:T(128)}, u32[]{:S(2)}) copy-start(s32[16]{0:T(128)} %param.23) | copy-start | bytes 196
  7.2 5.3 %copy-start.16 = (f32[8]{0:T(128)S(1)}, f32[8]{0:T(128)}, u32[]{:S(2)}) copy-start(f32[8]{0:T(128)} %param.28) | copy-start | bytes 100
  7.2 33.1 %all-reduce.2.cloned.1.call-start = ((), (), s32[]{:S(2)}) async-start(), calls=%async_computation.7 | async-start | bytes 131072 | tf_op jit(solution)/shard_map/psum | solution.py:100
  14.4 1.6 copy-start.1
  18.2 1.6 copy-start.1
  20.3 20.0 %copy-start.3 = (bf16[16,2048]{1,0:T(8,128)(2,1)S(1)}, bf16[16,2048]{1,0:T(8,128)(2,1)}, u32[]{:S(2)}) copy-start(bf16[16,2048]{1,0:T(8,128)(2,1)} %param.22) | copy-start | bytes 196612
  20.3 21.0 %copy-start.7 = (f32[2048]{0:T(1024)S(1)}, f32[2048]{0:T(1024)}, u32[]{:S(2)}) copy-start(f32[2048]{0:T(1024)} %param.32) | copy-start | bytes 24580
  20.3 21.0 %copy-start.11 = (f32[2048]{0:T(1024)S(1)}, f32[2048]{0:T(1024)}, u32[]{:S(2)}) copy-start(f32[2048]{0:T(1024)} %param.38) | copy-start | bytes 24580
  42.2 10.9 %all-to-all-start = ((bf16[16,16,128]{2,0,1:T(8,128)(2,1)}), bf16[16,16,128]{2,0,1:T(8,128)(2,1)S(1)}, u32[]{:S(2)}, u32[]{:S(2)}) async-start(bf16[16,16,128]{2,0,1:T(8,128)(2,1)} %bitcast.105), calls=%async_computation | async-start | bytes 131072 | tf_op jit(solution)/shard_map/all_to_all | solution.py:135
  49.0 9.6 %copy-start.5 = (bf16[128,256]{1,0:T(8,128)(2,1)S(1)}, bf16[128,256]{1,0:T(8,128)(2,1)}, u32[]{:S(2)}) copy-start(bf16[128,256]{1,0:T(8,128)(2,1)} %param.36) | copy-start | bytes 196612
  49.0 9.6 %copy-start.6 = (bf16[128,256]{1,0:T(8,128)(2,1)S(1)}, bf16[128,256]{1,0:T(8,128)(2,1)}, u32[]{:S(2)}) copy-start(bf16[128,256]{1,0:T(8,128)(2,1)} %param.35) | copy-start | bytes 196612
  53.1 28.3 %all-to-all-start.2 = ((bf16[16,12,2048]{2,1,0:T(8,128)(2,1)}), bf16[16,12,2048]{2,1,0:T(8,128)(2,1)S(1)}, u32[]{:S(2)}, u32[]{:S(2)}) async-start(bf16[16,12,2048]{2,1,0:T(8,128)(2,1)} %reshape.240), calls=%async_computation.4 | async-start | bytes 2097152 | tf_op jit(solution)/shard_map/all_to_all | solution.py:124
  58.5 63.7 %reduce-scatter.4.cloned.1.call-start = ((), (), s32[]{:S(2)}) async-start(), calls=%async_computation.8 | async-start | bytes 557056 | tf_op jit(solution)/shard_map/reduce_scatter | solution.py:137
  59.7 106.0 %reduce-scatter.8.cloned.1.call-start = ((), (), s32[]{:S(2)}) async-start(), calls=%async_computation.10 | async-start | bytes 1179648 | tf_op jit(solution)/shard_map/reduce_scatter | solution.py:63
  81.4 1.8 copy-start.12
  84.4 1.3 copy-start.10
  84.4 1.3 copy-start.13
  84.4 2.2 %copy-start.14 = (bf16[2048,64]{0,1:T(8,128)(2,1)S(1)}, bf16[2048,64]{0,1:T(8,128)(2,1)}, u32[]{:S(2)}) copy-start(bf16[2048,64]{0,1:T(8,128)(2,1)} %param.26) | copy-start | bytes 786436
  84.4 72.6 %copy-start.4 = (bf16[256,128]{1,0:T(8,128)(2,1)S(1)}, bf16[256,128]{1,0:T(8,128)(2,1)}, u32[]{:S(2)}) copy-start(bf16[256,128]{1,0:T(8,128)(2,1)} %param.37) | copy-start | bytes 196612
  84.4 80.8 %copy-start.15 = (bf16[2048,16]{0,1:T(8,128)(2,1)S(1)}, bf16[2048,16]{0,1:T(8,128)(2,1)}, u32[]{:S(2)}) copy-start(bf16[2048,16]{0,1:T(8,128)(2,1)} %param.33) | copy-start | bytes 196612
  157.8 12.0 %all-to-all-start.1 = ((bf16[16,16,128]{2,1,0:T(8,128)(2,1)}), bf16[16,16,128]{2,1,0:T(8,128)(2,1)S(1)}, u32[]{:S(2)}, u32[]{:S(2)}) async-start(bf16[16,16,128]{2,1,0:T(8,128)(2,1)} %bitcast.5), calls=%async_computation.2 | async-start | bytes 131072 | tf_op jit(solution)/shard_map/all_to_all | solution.py:152
  169.8 13.6 %all-to-all-start.3 = ((bf16[16,12,1024]{2,1,0:T(8,128)(2,1)}), bf16[16,12,1024]{2,1,0:T(8,128)(2,1)S(1)}, u32[]{:S(2)}, u32[]{:S(2)}) async-start(bf16[16,12,1024]{2,1,0:T(8,128)(2,1)} %copy.64), calls=%async_computation.6 | async-start | bytes 1048576 | tf_op jit(solution)/shard_map/all_to_all | solution.py:130
  175.1 31.7 %reduce-scatter.6.cloned.1.call-start = ((), (), s32[]{:S(2)}) async-start(), calls=%async_computation.9 | async-start | bytes 98304 | tf_op jit(solution)/shard_map/reduce_scatter | solution.py:155
  (2 other events, 2.4 us)
Sparse Core Ops, SparseCore 0:
  21.6 18.6 all-reduce.1
  61.6 60.6 reduce-scatter.3
  124.5 24.6 reduce-scatter.7
  177.8 28.9 reduce-scatter.5
where the time goes:
time: 218 us; the launch traced here: 215 us
  waiting for transfers between devices  109 us (50%)
  blocking collectives  34 us (16%)
  starting transfers between devices  24.8 us (11%)
  matrix products  16.5 us (8%)
  between operations  14.8 us (7%)
  local copies, waits for them, and re-layouts  8.55 us (4%)
  other arithmetic  6.76 us (3%)
    reduce_scatter x1, waiting for transfers between devices, shards(): lax.psum_scatter(jnp.dot(features2, paired_weights, preferred_element_typ...  34.8 us
    all_gather x1, blocking collectives, shards(): lax.all_gather(dense_hidden, 'ep', axis=0, tiled=True)  34 us
    reduce_scatter x1, waiting for transfers between devices, shards(): lax.psum_scatter(dense_partial, 'tp', scatter_dimension=1, tiled=True)  22.4 us
    all_to_all x1, waiting for transfers between devices, shards(): lax.all_to_all(send_rows, 'ep', split_axis=0, concat_axis=0, tiled=True)  21.6 us
    psum x1, waiting for transfers between devices, shards(): attn = lax.psum(attn_partial, 'tp').astype(jnp.float32)  18.2 us
    all_to_all x1, starting transfers between devices, shards(): lax.all_to_all(dense_columns.astype(jnp.bfloat16), 'ep', split_axis=0, co...  7.43 us
    all_to_all x1, waiting for transfers between devices, shards(): lax.all_to_all(summed, 'ep', split_axis=0, concat_axis=0, tiled=True)  7.38 us
    all_to_all x1, starting transfers between devices, shards(): lax.all_to_all(normed2, 'ep', split_axis=1, concat_axis=0, tiled=True)  6.42 us
  transfers between devices with their start and end apart: 8, of which 7 were waited for; matrix products, arithmetic and copies ran while one was open for 7% of the time, Pallas kernels for 0%

commit v1 on v0

v1 whole, which is shorter than its diff:
```python
import functools

import jax
import jax.numpy as jnp
from jax import lax
from jax.experimental import pallas as pl
from jax.experimental.pallas import tpu as pltpu
from jax.sharding import PartitionSpec as P


def rms_scale(values, gain):
    wide = values.astype(jnp.float32)
    return wide * lax.rsqrt(jnp.mean(wide * wide, axis=-1, keepdims=True) + 1e-06) * gain


def stick_read(queries, lengths, head_bias, key_cache, value_cache):
    seq_count, local_kv, head_dim, cache_len = key_cache.shape
    group_size = head_bias.shape[0] // local_kv
    grouped = queries.reshape(seq_count, local_kv, group_size, head_dim)
    head_shift = head_bias.reshape(1, local_kv, group_size, 1)
    span_len = min(512, cache_len)
    block_count = (jnp.max(lengths) + span_len - 1) // span_len
    span_index = lax.iota(jnp.int32, span_len)
    after_mask = (span_index[:, None] > span_index[None, :]).astype(jnp.float32)

    def visit(visit_index, carry):
        totals, log_later = carry
        first = (block_count - 1 - visit_index) * span_len
        key_block = lax.dynamic_slice_in_dim(key_cache, first, span_len, 3)
        value_block = lax.dynamic_slice_in_dim(value_cache, first, span_len, 3)
        scores = (
            jnp.einsum("skgd,skdc->skgc", grouped, key_block, preferred_element_type=jnp.float32)
            * head_dim ** (-0.5)
            + head_shift
        )
        positions = first + span_index
        visible = (positions[None, :] < lengths[:, None])[:, None, None, :]
        log_keep = jnp.where(visible, jax.nn.log_sigmoid(-scores), 0.0)
        log_after = (
            jnp.einsum("skgj,jc->skgc", log_keep, after_mask, precision=lax.Precision.HIGHEST)
            + log_later[..., None]
        )
        weights = jnp.where(visible, jnp.exp(jax.nn.log_sigmoid(scores) + log_after), 0.0).astype(
            jnp.bfloat16
        )
        totals = totals + jnp.einsum(
            "skgc,skdc->skgd", weights, value_block, preferred_element_type=jnp.float32
        )
        return (totals, log_later + jnp.sum(log_keep, axis=3))

    start_totals = jnp.zeros((seq_count, local_kv, group_size, head_dim), jnp.float32)
    start_later = jnp.zeros((seq_count, local_kv, group_size), jnp.float32)
    totals, unused_later = lax.fori_loop(0, block_count, visit, (start_totals, start_later))
    return totals.reshape(seq_count, -1).astype(jnp.bfloat16)


MESH = pl.DeviceIdType.MESH


def after_attention(
    n,
    width,
    heads_ref,
    tokens_ref,
    gain_ref,
    router_ref,
    routes_ref,
    mix_ref,
    paired_ref,
    down_ref,
    w_out_hbm,
    w_gate_hbm,
    w_up_hbm,
    w_down_hbm,
    out_ref,
    w_out,
    w_gate,
    w_up,
    w_down,
    load_sem,
    attn_mine,
    attn_peer,
    res_ref,
    norm_all,
    part_send,
    part_recv,
    hidden_ref,
    dense_all,
    cols_send,
    cols_recv,
    other_ref,
    mine_ref,
    peer_ref,
    back_send,
    back_recv,
    pair_sems,
    norm_sems,
    pass_sems,
    part_sems,
    dense_sems,
    cols_send_sem,
    cols_recv_sem,
    back_sems,
):
    me = lax.axis_index("ep")
    core = lax.axis_index("tp")
    peer = 1 - core
    rows, model = tokens_ref.shape
    half = model // 2
    window = paired_ref.shape[0]
    first = (me * width) // window * window
    owner = first // half
    lane = pl.multiple_of(first % half, window)
    f32 = jnp.float32

    def remote(source, target, send_sem, recv_sem, ep, tp):
        return pltpu.make_async_remote_copy(
            src_ref=source,
            dst_ref=target,
            send_sem=send_sem,
            recv_sem=recv_sem,
            device_id=(ep, tp),
            device_id_type=MESH,
        )

    loads = [
        pltpu.make_async_copy(source, target, load_sem.at[i])
        for i, (source, target) in enumerate(
            ((w_out_hbm, w_out), (w_gate_hbm, w_gate), (w_up_hbm, w_up), (w_down_hbm, w_down))
        )
    ]
    for load in loads:
        load.start()

    barrier = pltpu.get_barrier_semaphore()

    def greet(k, carry):
        other = lax.rem(me + k, n)
        pl.semaphore_signal(barrier, inc=1, device_id=(other, core), device_id_type=MESH)
        pl.semaphore_signal(barrier, inc=1, device_id=(other, peer), device_id_type=MESH)
        return carry

    lax.fori_loop(1, n, greet, 0)
    pl.semaphore_signal(barrier, inc=1, device_id=(me, peer), device_id_type=MESH)

    loads[0].wait()
    attn_mine[...] = jnp.dot(heads_ref[...], w_out[...], preferred_element_type=f32).astype(
        jnp.bfloat16
    )
    pl.semaphore_wait(barrier, 2 * n - 1)

    swap = remote(attn_mine, attn_peer, pair_sems.at[0], pair_sems.at[1], me, peer)
    swap.start()
    swap.wait()
    attn = attn_mine[...].astype(f32) + attn_peer[...].astype(f32)
    residual = (tokens_ref[...].astype(f32) + attn).astype(jnp.bfloat16)
    res_ref[...] = residual
    wide = residual.astype(f32)
    normed = (
        wide * lax.rsqrt(jnp.mean(wide * wide, axis=-1, keepdims=True) + 1e-06) * gain_ref[...]
    ).astype(jnp.bfloat16)
    norm_all[0, me] = normed[:, :half]
    norm_all[1, me] = normed[:, half:]

    def norm_copy(j, other):
        return remote(
            norm_all.at[core, j],
            norm_all.at[core, j],
            norm_sems.at[0, other],
            norm_sems.at[1, j],
            other,
            core,
        )

    def pass_copy(j, which):
        return remote(
            norm_all.at[which, j],
            norm_all.at[which, j],
            pass_sems.at[0, j],
            pass_sems.at[1, j],
            me,
            peer,
        )

    def send_norm(k, carry):
        norm_copy(me, lax.rem(me + k, n)).start()
        return carry

    lax.fori_loop(1, n, send_norm, 0)

    probs = jax.nn.sigmoid(jnp.dot(normed, router_ref[...], preferred_element_type=f32))
    expert_total = probs.shape[1]
    expert_index = lax.broadcasted_iota(jnp.int32, (rows, expert_total), 1)
    hits = jnp.zeros((rows, expert_total), f32)
    for k in range(routes_ref.shape[1]):
        hits = jnp.where(routes_ref[:, k : k + 1] == expert_index, 1.0, hits)
    picked = jnp.where(hits > 0.0, probs, 0.0)
    gates = picked / jnp.sum(picked, axis=-1, keepdims=True) * 2.5
    mix_gate = jax.nn.sigmoid(
        jnp.sum(normed.astype(f32) * mix_ref[...], axis=-1, keepdims=True)
    )

    def take_norm(k, carry):
        j = lax.rem(me + n - k, n)
        norm_copy(j, me).wait_recv()
        pass_copy(j, core).start()
        return carry

    lax.fori_loop(1, n, take_norm, 0)

    def take_pass(k, carry):
        pass_copy(lax.rem(me + n - k, n), peer).wait_recv()
        return carry

    lax.fori_loop(1, n, take_pass, 0)

    def part_copy(j, other):
        return remote(
            part_send.at[other],
            part_recv.at[j],
            part_sems.at[0, other],
            part_sems.at[1, j],
            other,
            core,
        )

    def back_copy(j, other):
        return remote(
            back_send.at[other],
            back_recv.at[j],
            back_sems.at[0, other],
            back_sems.at[1, j],
            other,
            core,
        )

    def dense_copy(j, other):
        return remote(
            dense_all.at[j],
            dense_all.at[j],
            dense_sems.at[0, other],
            dense_sems.at[1, j],
            other,
            core,
        )

    group = min(n, 16)
    groups = n // group
    block = group * rows

    def dense_first(c, carry):
        base = c * group
        features = norm_all[owner, pl.ds(base, group), :, pl.ds(lane, window)]
        value = jnp.dot(
            features.reshape(block, window), paired_ref[...], preferred_element_type=f32
        )
        part_send[pl.ds(base, group)] = value.astype(jnp.bfloat16).reshape(group, rows, -1)
        return carry

    lax.fori_loop(0, groups, dense_first, 0)

    def send_part(k, carry):
        part_copy(me, lax.rem(me + k, n)).start()
        return carry

    lax.fori_loop(1, n, send_part, 0)

    loads[1].wait()
    loads[2].wait()

    def expert_first(c, carry):
        base = c * group
        low = norm_all[0, pl.ds(base, group)].reshape(block, half)
        high = norm_all[1, pl.ds(base, group)].reshape(block, half)
        gate_rows = jnp.dot(low, w_gate[:half], preferred_element_type=f32) + jnp.dot(
            high, w_gate[half:], preferred_element_type=f32
        )
        up_rows = jnp.dot(low, w_up[:half], preferred_element_type=f32) + jnp.dot(
            high, w_up[half:], preferred_element_type=f32
        )
        hidden_ref[pl.ds(c, 1)] = (jax.nn.silu(gate_rows) * up_rows).astype(jnp.bfloat16)[None]
        return carry

    lax.fori_loop(0, groups, expert_first, 0)

    def take_part(k, total):
        j = lax.rem(me + n - k, n)
        part_copy(j, me).wait_recv()
        return total + part_recv[j].astype(f32)

    paired = lax.fori_loop(1, n, take_part, part_send[me].astype(f32))
    hidden_cols = paired.shape[1] // 2
    dense_all[me] = (jax.nn.silu(paired[:, :hidden_cols]) * paired[:, hidden_cols:]).astype(
        jnp.bfloat16
    )

    def send_dense(k, carry):
        dense_copy(me, lax.rem(me + k, n)).start()
        return carry

    lax.fori_loop(1, n, send_dense, 0)

    loads[3].wait()
    far = pl.ds(pl.multiple_of(peer * half, half), half)
    near = pl.ds(pl.multiple_of(core * half, half), half)

    def expert_far(c, carry):
        value = jnp.dot(hidden_ref[c], w_down[:, far], preferred_element_type=f32)
        other_ref[pl.ds(c * group, group)] = value.astype(jnp.bfloat16).reshape(group, rows, half)
        return carry

    lax.fori_loop(0, groups, expert_far, 0)
    trade = remote(other_ref, peer_ref, pair_sems.at[2], pair_sems.at[3], me, peer)
    trade.start()

    def expert_near(c, carry):
        value = jnp.dot(hidden_ref[c], w_down[:, near], preferred_element_type=f32)
        mine_ref[pl.ds(c * group, group)] = value.astype(jnp.bfloat16).reshape(group, rows, half)
        return carry

    lax.fori_loop(0, groups, expert_near, 0)
    trade.wait()

    def send_back(k, carry):
        other = lax.rem(me + k, n)
        total = mine_ref[other].astype(f32) + peer_ref[other].astype(f32)
        back_send[other] = total.astype(jnp.bfloat16)

        @pl.when(k > 0)
        def _():
            back_copy(me, other).start()

        return carry

    lax.fori_loop(0, n, send_back, 0)

    def take_dense(k, carry):
        dense_copy(lax.rem(me + n - k, n), me).wait_recv()
        return carry

    lax.fori_loop(1, n, take_dense, 0)

    def dense_second(c, carry):
        base = c * group
        value = jnp.dot(
            dense_all[pl.ds(base, group)].reshape(block, hidden_cols),
            down_ref[...],
            preferred_element_type=f32,
        )
        cols_send[pl.ds(base, group)] = value.astype(jnp.bfloat16).reshape(group, rows, window)
        return carry

    lax.fori_loop(0, groups, dense_second, 0)

    def cols_copy(from_core, j, other, target):
        return remote(
            cols_send.at[other],
            cols_recv.at[from_core, j],
            cols_send_sem.at[other],
            cols_recv_sem.at[from_core, j],
            other,
            target,
        )

    def send_cols(k, carry):
        cols_copy(core, me, lax.rem(me + k, n), owner).start()
        return carry

    lax.fori_loop(1, n, send_cols, 0)

    @pl.when(owner == core)
    def _():
        cols_recv[core, me] = cols_send[me]

    @pl.when(owner != core)
    def _():
        cols_copy(core, me, me, peer).start()

    def take_cols(k, carry):
        j = core * (n // 2) + k

        @pl.when(j != me)
        def _():
            cols_copy(core, j, me, core).wait_recv()

        cols_copy(peer, j, me, core).wait_recv()
        return carry

    lax.fori_loop(0, n // 2, take_cols, 0)
    per_window = window // width
    dense_parts = []
    for q in range(half // window):
        total = jnp.zeros((rows, window), f32)
        for r in range(per_window):
            j = core * (n // 2) + q * per_window + r
            total = total + cols_recv[0, j].astype(f32) + cols_recv[1, j].astype(f32)
        dense_parts.append(total)
    dense = jnp.concatenate(dense_parts, axis=1)
    total = res_ref[:, near].astype(f32) + mix_gate * dense

    def take_back(k, total):
        j = lax.rem(me + n - k, n)

        @pl.when(k > 0)
        def _():
            back_copy(j, me).wait_recv()

        @pl.when(k == 0)
        def _():
            back_recv[me] = back_send[me]

        gate = jnp.sum(jnp.where(expert_index == j, gates, 0.0), axis=-1, keepdims=True)
        return total + gate * back_recv[j].astype(f32)

    out_ref[...] = lax.fori_loop(0, n, take_back, total).astype(jnp.bfloat16)

    def drain(k, carry):
        other = lax.rem(me + k, n)
        norm_copy(me, other).wait_send()
        pass_copy(other, core).wait_send()
        part_copy(me, other).wait_send()
        dense_copy(me, other).wait_send()
        cols_copy(core, me, other, owner).wait_send()
        back_copy(me, other).wait_send()
        return carry

    lax.fori_loop(1, n, drain, 0)

    @pl.when(owner != core)
    def _():
        cols_copy(core, me, me, peer).wait_send()


def shards(
    n,
    tokens,
    lengths,
    attn_gain,
    w_query,
    w_key,
    w_value,
    head_bias,
    key_cache,
    value_cache,
    w_attn_out,
    ffn_gain,
    w_router,
    routes,
    w_dense_gate,
    w_dense_up,
    w_dense_down,
    dense_mix,
    w_expert_gate,
    w_expert_up,
    w_expert_down,
):
    rows, model = tokens.shape
    half = model // 2
    normed = rms_scale(tokens, attn_gain).astype(jnp.bfloat16)
    new_keys = jnp.dot(normed, w_key, preferred_element_type=jnp.float32).astype(jnp.bfloat16)
    new_values = jnp.dot(normed, w_value, preferred_element_type=jnp.float32).astype(jnp.bfloat16)
    queries = jnp.dot(normed, w_query, preferred_element_type=jnp.float32).astype(jnp.bfloat16)
    heads_out = stick_read(queries, lengths, head_bias, key_cache, value_cache)

    width, hidden_cols = w_dense_gate.shape
    window = max(width, 128)
    paired = jnp.concatenate([w_dense_gate, w_dense_up], axis=1)
    down = w_dense_down
    if window != width:
        shift = (lax.axis_index("ep") * width) % window
        paired = lax.dynamic_update_slice(
            jnp.zeros((window, paired.shape[1]), paired.dtype), paired, (shift, 0)
        )
        down = lax.dynamic_update_slice(
            jnp.zeros((hidden_cols, window), down.dtype), down, (0, shift)
        )
    w_gate, w_up, w_down = w_expert_gate[0], w_expert_up[0], w_expert_down[0]
    expert_hidden = w_gate.shape[1]
    bf16 = jnp.bfloat16
    block = min(n, 16) * rows
    vmem = pl.BlockSpec(memory_space=pltpu.VMEM)
    anywhere = pl.BlockSpec(memory_space=pl.ANY)
    dma = pltpu.SemaphoreType.DMA
    layer_out = pl.pallas_call(
        functools.partial(after_attention, n, width),
        out_shape=jax.ShapeDtypeStruct((rows, half), bf16),
        in_specs=[vmem] * 8 + [anywhere] * 4,
        out_specs=vmem,
        scratch_shapes=[
            pltpu.VMEM(w_attn_out.shape, bf16),
            pltpu.VMEM(w_gate.shape, bf16),
            pltpu.VMEM(w_up.shape, bf16),
            pltpu.VMEM(w_down.shape, bf16),
            dma((4,)),
            pltpu.VMEM((rows, model), bf16),
            pltpu.VMEM((rows, model), bf16),
            pltpu.VMEM((rows, model), bf16),
            pltpu.VMEM((2, n, rows, half), bf16),
            pltpu.VMEM((n, rows, 2 * hidden_cols), bf16),
            pltpu.VMEM((n, rows, 2 * hidden_cols), bf16),
            pltpu.VMEM((n * rows // block, block, expert_hidden), bf16),
            pltpu.VMEM((n, rows, hidden_cols), bf16),
            pltpu.VMEM((n, rows, window), bf16),
            pltpu.VMEM((2, n, rows, window), bf16),
            pltpu.VMEM((n, rows, half), bf16),
            pltpu.VMEM((n, rows, half), bf16),
            pltpu.VMEM((n, rows, half), bf16),
            pltpu.VMEM((n, rows, half), bf16),
            pltpu.VMEM((n, rows, half), bf16),
            dma((4,)),
            dma((2, n)),
            dma((2, n)),
            dma((2, n)),
            dma((2, n)),
            dma((n,)),
            dma((2, n)),
            dma((2, n)),
        ],
        compiler_params=pltpu.CompilerParams(
            collective_id=0, has_side_effects=True, vmem_limit_bytes=48 * 1024 * 1024
        ),
        name="after_attention",
    )(
        heads_out,
        tokens,
        ffn_gain.reshape(1, model),
        w_router,
        routes,
        dense_mix.reshape(1, model),
        paired,
        down,
        w_attn_out,
        w_gate,
        w_up,
        w_down,
    )
    return (layer_out, new_keys, new_values)


def solution(mesh):
    return jax.shard_map(
        functools.partial(shards, mesh.shape["ep"]),
        mesh=mesh,
        in_specs=(
            P("ep", None),
            P("ep"),
            P(),
            P(None, "tp"),
            P(None, "tp"),
            P(None, "tp"),
            P("tp"),
            P("ep", "tp", None, None),
            P("ep", "tp", None, None),
            P("tp", None),
            P(),
            P(),
            P("ep", None),
            P("ep", "tp"),
            P("ep", "tp"),
            P("tp", "ep"),
            P(),
            P("ep", None, "tp"),
            P("ep", None, "tp"),
            P("ep", "tp", None),
        ),
        out_specs=(P("ep", "tp"), P("ep", "tp"), P("ep", "tp")),
        check_vma=False,
    )
```

time: 218 us -> 72.5 us (0.33)
  the two profiles are of different devices: /device:TPU:7 before, /device:TPU:1 now
where the time goes in v1:
time: 72.5 us; the launch traced here: 72 us
  Pallas kernels  54.7 us (75%)
  local copies, waits for them, and re-layouts  7.32 us (10%)
  matrix products  5.87 us (8%)
  other arithmetic  2.53 us (3%)
  between operations  1.54 us (2%)
    pallas_call x1, Pallas kernels, shards(): pl.pallas_call(functools.partial(after_attention, n, width), out_shape=ja...  54.7 us
    unnamed x39, local copies, waits for them, and re-layouts  6.31 us
    dot_general x1, matrix products, visit(): jnp.einsum('skgd,skdc->skgc', grouped, key_block, preferred_element_type=...  1.64 us

profile of v1, /device:TPU:1, one launch (start us, length us, event | category | flops | bytes accessed | tf_op | source)
XLA Modules:
  0.0 72.0 jit_solution(15742656505560386068)
XLA Ops:
  0.6 0.0 copy-start
  0.7 1.4 %reduce_max.9 = s32[]{:T(128)} reduce(s32[16]{0:T(128)} %param.23, s32[]{:T(128)} %constant.55.clone.1), dimensions={0}, to_apply=%region_0.0 | reduce | flops 15 | bytes 72 | tf_op jit(solution)/shard_map/reduce_max | solution.py:22
  2.8 1.0 %fusion.27 = f32[16]{0:T(128)S(1)} fusion(bf16[16,2048]{1,0:T(8,128)(2,1)} %tokens_ref.1), kind=kLoop, calls=%fused_computation.38 | loop fusion | flops 98288 | bytes 65600 | tf_op jit(solution)/shard_map/reduce_sum | solution.py:13
  3.8 1.3 %convolution_convert_fusion = bf16[16,512]{1,0:T(8,128)(2,1)S(1)} fusion(bf16[2048,512]{1,0:T(8,128)(2,1)S(1)} %copy-done, bf16[16,2048]{1,0:T(8,128)(2,1)} %tokens_ref.1, f32[2048]{0:T(1024)} %param.24, f32[16]{0:T(128)S(1)} %add_rsqrt_fusion), kind=kOutput, calls=%fused_computation.33 | convolution fusion | flops 33693696 | bytes 2187328 | tf_op jit(solution)/shard_map/dot_general | solution.py:462
  5.0 0.1 reshape.123
  5.3 3.9 %while.15 = (s32[]{:T(128)}, f32[16,1,8,64]{3,2,0,1:T(8,128)S(1)}, f32[16,1,8]{0,2,1:T(8,128)S(1)}, s32[]{:T(128)}, s32[]{:T(128)}, /*index=5*/s32[16]{0:T(128)S...) while((s32[]{:T(128)}, f32[16,1,8,64]{3,2,0,1:T(8,128)S(1)}, ...), condition=%wide.region_4.5_spmd.clone, body=%wide.region_2.4_spmd.clone.sunk | while | flops 422003200 | bytes 11420487 | solution.py:53
  5.3 0.1 broadcast_compare_fusion.2
  5.4 1.6 %fusion.48 = (f32[16,8]{1,0:T(8,128)S(1)}, f32[16,8,512]{2,1,0:T(8,128)S(1)}) fusion(pred[16,512]{1,0:T(8,128)(4,1)S(1)} %broadcast_compare_fusion.2, f32[8]{0:T(128)S(1)} %bitcast.69, bf16[16,1,8,64]{3,2,0,1:T(8,128)(2,1)S(1)} %get-tuple-element.306, bf16[16,1,64,1024]{3,2,0,1:T(8,128)(2,1)} %get-tuple-element.305, s32[]{:T(128)S(6)} %select_n.77), kind=kOutput, calls=%fused_computation.24.clone.1 | convolution fusion | flops 9109376 | bytes 1335844 | tf_op jit(solution)/shard_map/while/body/skgd,skdc->skgc/dot_general | solution.py:32
  7.0 0.1 copy.36
  7.1 0.9 %fusion.49 = bf16[16,8,512]{2,1,0:T(8,128)(2,1)S(1)} fusion(f32[16,8,512]{2,1,0:T(8,128)S(1)} %get-tuple-element.269, f32[16,8]{1,0:T(8,128)S(1)} %copy.36, pred[16,512]{1,0:T(8,128)(4,1)S(1)} %broadcast_compare_fusion.2), kind=kOutput, calls=%fused_computation.9.clone.1 | convolution fusion | flops 404488192 | bytes 401920 | tf_op jit(solution)/shard_map/while/body/skgj,jc->skgc/dot_general | solution.py:40
  8.0 0.7 copy-done.9
  8.7 0.4 fusion.50
  9.1 0.1 copy.37
  9.2 0.1 convert_element_type.34.heads_ref
  9.3 0.3 copy.32.router_ref
  9.6 0.1 copy.33.routes_ref
  9.7 1.6 %copy-done.1 = bf16[512,2048]{1,0:T(8,128)(2,1)S(1)} copy-done((bf16[512,2048]{1,0:T(8,128)(2,1)S(1)}, bf16[512,2048]{1,0:T(8,128)(2,1)}, u32[]{:S(2)}) %copy-start.1) | copy-done | bytes 2097176
  11.3 1.2 %copy-done.2 = bf16[1,2048,256]{2,1,0:T(8,128)(2,1)S(1)} copy-done((bf16[1,2048,256]{2,1,0:T(8,128)(2,1)S(1)}, bf16[1,2048,256]{2,1,0:T(8,128)(2,1)}, u32[]{:S(2)}) %copy-start.2) | copy-done | bytes 1048600
  12.5 1.2 %copy-done.3 = bf16[1,2048,256]{2,1,0:T(8,128)(2,1)S(1)} copy-done((bf16[1,2048,256]{2,1,0:T(8,128)(2,1)S(1)}, bf16[1,2048,256]{2,1,0:T(8,128)(2,1)}, u32[]{:S(2)}) %copy-start.3) | copy-done | bytes 1048600
  13.8 1.2 %copy-done.4 = bf16[1,256,2048]{2,1,0:T(8,128)(2,1)S(1)} copy-done((bf16[1,256,2048]{2,1,0:T(8,128)(2,1)S(1)}, bf16[1,256,2048]{2,1,0:T(8,128)(2,1)}, u32[]{:S(2)}) %copy-start.4) | copy-done | bytes 1048600
  15.0 54.7 %after_attention.1 = bf16[16,1024]{1,0:T(8,128)(2,1)S(1)} custom-call(bf16[16,512]{1,0:T(8,128)(2,1)S(1)} %convert_element_type.34.heads_ref, bf16[16,2048]{1,0:T(8,128)(2,1)S(1)} %copy-done.5, f32[1,2048]{1,0:T(1,128)S(1)} %bitcast.63, bf16[2048,16]{1,0:T(8,128)(2,1)S(1)} %copy.32.router_ref, s32[16,6]{1,0:T(8,128)S(1)} %copy.33.routes_ref, ...), custom_call_target="tpu_custom_call" | custom-call | tf_op jit(solution)/shard_map/after_attention/pallas_call | solution.py:484
  69.7 0.8 %convolution_convert_fusion.1 = bf16[16,64]{1,0:T(8,128)(2,1)} fusion(bf16[2048,64]{0,1:T(8,128)(2,1)S(1)} %copy-done.16, bf16[16,2048]{1,0:T(8,128)(2,1)S(1)} %copy-done.5, f32[2048]{0:T(1024)S(1)} %copy-done.14, f32[16]{0:T(128)S(1)} %add_rsqrt_fusion), kind=kOutput, calls=%fused_computation.34 | convolution fusion | flops 4326400 | bytes 337984 | tf_op jit(solution)/shard_map/dot_general | solution.py:461
  70.6 0.8 %convolution_convert_fusion.2 = bf16[16,64]{1,0:T(8,128)(2,1)} fusion(bf16[2048,64]{0,1:T(8,128)(2,1)S(1)} %copy-done.17, bf16[16,2048]{1,0:T(8,128)(2,1)S(1)} %copy-done.5, f32[2048]{0:T(1024)S(1)} %copy-done.14, f32[16]{0:T(128)S(1)} %add_rsqrt_fusion), kind=kOutput, calls=%fused_computation.35 | convolution fusion | flops 4326400 | bytes 337984 | tf_op jit(solution)/shard_map/dot_general | solution.py:460
  71.4 0.6 copy.48
  (39 shorter events, 0.1 us)
Async XLA Ops:
  0.6 3.1 %copy-start = (bf16[2048,512]{1,0:T(8,128)(2,1)S(1)}, bf16[2048,512]{1,0:T(8,128)(2,1)}, u32[]{:S(2)}) copy-start(bf16[2048,512]{1,0:T(8,128)(2,1)} %param.25) | copy-start | bytes 6291460
  0.6 4.5 %copy-start.13 = (s32[16]{0:T(128)S(1)}, s32[16]{0:T(128)}, u32[]{:S(2)}) copy-start(s32[16]{0:T(128)} %param.23) | copy-start | bytes 196
  0.7 4.5 %copy-start.18 = (f32[8]{0:T(128)S(1)}, f32[8]{0:T(128)}, u32[]{:S(2)}) copy-start(f32[8]{0:T(128)} %param.28) | copy-start | bytes 100
  5.2 4.1 %copy-start.10 = (bf16[2048,16]{0,1:T(8,128)(2,1)S(1)}, bf16[2048,16]{0,1:T(8,128)(2,1)}, u32[]{:S(2)}) copy-start(bf16[2048,16]{0,1:T(8,128)(2,1)} %param.33) | copy-start | bytes 196612
  5.2 4.4 %copy-start.11 = (bf16[128,256]{1,0:T(8,128)(2,1)S(1)}, bf16[128,256]{1,0:T(8,128)(2,1)}, u32[]{:S(2)}) copy-start(bf16[128,256]{1,0:T(8,128)(2,1)} %param.36) | copy-start | bytes 196612
  5.2 4.4 %copy-start.12 = (bf16[128,256]{1,0:T(8,128)(2,1)S(1)}, bf16[128,256]{1,0:T(8,128)(2,1)}, u32[]{:S(2)}) copy-start(bf16[128,256]{1,0:T(8,128)(2,1)} %param.35) | copy-start | bytes 196612
  5.2 4.4 %copy-start.15 = (s32[16,6]{0,1:T(8,128)S(1)}, s32[16,6]{0,1:T(8,128)}, u32[]{:S(2)}) copy-start(s32[16,6]{0,1:T(8,128)} %param.34) | copy-start | bytes 1156
  5.2 4.5 %copy-start.5 = (bf16[16,2048]{1,0:T(8,128)(2,1)S(1)}, bf16[16,2048]{1,0:T(8,128)(2,1)}, u32[]{:S(2)}) copy-start(bf16[16,2048]{1,0:T(8,128)(2,1)} %tokens_ref.1) | copy-start | bytes 196612
  5.2 4.5 %copy-start.6 = (bf16[256,128]{1,0:T(8,128)(2,1)S(1)}, bf16[256,128]{1,0:T(8,128)(2,1)}, u32[]{:S(2)}) copy-start(bf16[256,128]{1,0:T(8,128)(2,1)} %down_ref.1) | copy-start | bytes 196612
  5.2 4.4 %copy-start.7 = (f32[2048]{0:T(1024)S(1)}, f32[2048]{0:T(1024)}, u32[]{:S(2)}) copy-start(f32[2048]{0:T(1024)} %param.32) | copy-start | bytes 24580
  5.3 4.4 %copy-start.8 = (f32[2048]{0:T(1024)S(1)}, f32[2048]{0:T(1024)}, u32[]{:S(2)}) copy-start(f32[2048]{0:T(1024)} %param.38) | copy-start | bytes 24580
  7.1 1.6 %copy-start.9 = (bf16[16,1,64,1024]{3,2,0,1:T(8,128)(2,1)S(1)}, bf16[16,1,64,1024]{3,2,0,1:T(8,128)(2,1)}, u32[]{:S(2)}) copy-start(bf16[16,1,64,1024]{3,2,0,1:T(8,128)(2,1)} %get-tuple-element.308) | copy-start | bytes 6291460 | tf_op jit(solution)/shard_map/while
  9.7 1.6 %copy-start.1 = (bf16[512,2048]{1,0:T(8,128)(2,1)S(1)}, bf16[512,2048]{1,0:T(8,128)(2,1)}, u32[]{:S(2)}) copy-start(bf16[512,2048]{1,0:T(8,128)(2,1)} %w_out_hbm.1) | copy-start | bytes 6291460
  11.3 1.2 %copy-start.2 = (bf16[1,2048,256]{2,1,0:T(8,128)(2,1)S(1)}, bf16[1,2048,256]{2,1,0:T(8,128)(2,1)}, u32[]{:S(2)}) copy-start(bf16[1,2048,256]{2,1,0:T(8,128)(2,1)} %param.39) | copy-start | bytes 3145732
  12.5 1.2 %copy-start.3 = (bf16[1,2048,256]{2,1,0:T(8,128)(2,1)S(1)}, bf16[1,2048,256]{2,1,0:T(8,128)(2,1)}, u32[]{:S(2)}) copy-start(bf16[1,2048,256]{2,1,0:T(8,128)(2,1)} %param.40) | copy-start | bytes 3145732
  13.8 1.2 %copy-start.4 = (bf16[1,256,2048]{2,1,0:T(8,128)(2,1)S(1)}, bf16[1,256,2048]{2,1,0:T(8,128)(2,1)}, u32[]{:S(2)}) copy-start(bf16[1,256,2048]{2,1,0:T(8,128)(2,1)} %param.41) | copy-start | bytes 3145732
  15.0 54.7 %copy-start.14 = (f32[2048]{0:T(1024)S(1)}, f32[2048]{0:T(1024)}, u32[]{:S(2)}) copy-start(f32[2048]{0:T(1024)} %param.24) | copy-start | bytes 24580
  15.0 54.7 %copy-start.16 = (bf16[2048,64]{0,1:T(8,128)(2,1)S(1)}, bf16[2048,64]{0,1:T(8,128)(2,1)}, u32[]{:S(2)}) copy-start(bf16[2048,64]{0,1:T(8,128)(2,1)} %param.27) | copy-start | bytes 786436
  15.0 55.6 %copy-start.17 = (bf16[2048,64]{0,1:T(8,128)(2,1)S(1)}, bf16[2048,64]{0,1:T(8,128)(2,1)}, u32[]{:S(2)}) copy-start(bf16[2048,64]{0,1:T(8,128)(2,1)} %param.26) | copy-start | bytes 786436

commit v2 on v1

v2 whole, which is shorter than its diff:
```python
import functools

import jax
import jax.numpy as jnp
from jax import lax
from jax.experimental import pallas as pl
from jax.experimental.pallas import tpu as pltpu
from jax.sharding import PartitionSpec as P

MESH = pl.DeviceIdType.MESH


def whole_layer(
    n,
    group_size,
    tokens_ref,
    attn_gain_ref,
    limits_ref,
    bias_ref,
    w_key_ref,
    w_value_ref,
    gain_ref,
    router_ref,
    routes_ref,
    mix_ref,
    paired_ref,
    down_ref,
    w_query_hbm,
    w_out_hbm,
    w_gate_hbm,
    w_up_hbm,
    w_down_hbm,
    keys_hbm,
    values_hbm,
    out_ref,
    new_keys_ref,
    new_values_ref,
    w_query,
    w_out,
    w_gate,
    w_up,
    w_down,
    keys,
    values,
    load_sem,
    keys_sem,
    values_sem,
    query_ref,
    score_ref,
    read_ref,
    normed_ref,
    paired_all,
    down_all,
    attn_mine,
    attn_peer,
    res_ref,
    norm_all,
    part_send,
    part_recv,
    hidden_ref,
    dense_all,
    cols_send,
    cols_recv,
    other_ref,
    mine_ref,
    peer_ref,
    back_send,
    back_recv,
    pair_sems,
    paired_sems,
    down_sems,
    norm_sems,
    pass_sems,
    part_sems,
    dense_sems,
    cols_send_sem,
    cols_recv_sem,
    back_sems,
):
    me = lax.axis_index("ep")
    core = lax.axis_index("tp")
    peer = 1 - core
    rows, model = tokens_ref.shape
    half = model // 2
    width = paired_ref.shape[0]
    window = width * group_size
    place = me % group_size
    team = me // group_size
    teams = n // group_size
    first = team * window
    owner = first // half
    lane = pl.multiple_of(first % half, window)
    f32 = jnp.float32
    local_heads = bias_ref.shape[0]
    head_dim, cache_len = keys_hbm.shape[1:]
    span = 4

    def remote(source, target, send_sem, recv_sem, ep, tp):
        return pltpu.make_async_remote_copy(
            src_ref=source,
            dst_ref=target,
            send_sem=send_sem,
            recv_sem=recv_sem,
            device_id=(ep, tp),
            device_id_type=MESH,
        )

    pairs = (
        (w_query_hbm, w_query),
        (w_gate_hbm, w_gate),
        (w_up_hbm, w_up),
        (w_down_hbm, w_down),
        (w_out_hbm, w_out),
    )
    loads = [
        pltpu.make_async_copy(source, target, load_sem.at[i])
        for i, (source, target) in enumerate(pairs)
    ]

    def keys_load(c):
        block = pl.ds(c * span, span)
        return pltpu.make_async_copy(keys_hbm.at[block], keys.at[block], keys_sem.at[c])

    def values_load(c):
        block = pl.ds(c * span, span)
        return pltpu.make_async_copy(values_hbm.at[block], values.at[block], values_sem.at[c])

    loads[0].start()
    for c in range(rows // span):
        keys_load(c).start()
        values_load(c).start()
    for load in (loads[4], loads[1], loads[2], loads[3]):
        load.start()

    barrier = pltpu.get_barrier_semaphore()

    def greet(k, carry):
        other = lax.rem(me + k, n)
        pl.semaphore_signal(barrier, inc=1, device_id=(other, core), device_id_type=MESH)
        pl.semaphore_signal(barrier, inc=1, device_id=(other, peer), device_id_type=MESH)
        return carry

    lax.fori_loop(1, n, greet, 0)
    pl.semaphore_signal(barrier, inc=1, device_id=(me, peer), device_id_type=MESH)

    start = tokens_ref[...].astype(f32)
    normed_ref[...] = (
        start
        * lax.rsqrt(jnp.mean(start * start, axis=-1, keepdims=True) + 1e-06)
        * attn_gain_ref[...]
    ).astype(jnp.bfloat16)
    loads[0].wait()
    queries = jnp.dot(normed_ref[...], w_query[...], preferred_element_type=f32)
    queries = queries.astype(jnp.bfloat16).astype(f32)
    for h in range(local_heads):
        query_ref[:, h, :] = queries[:, h * head_dim : (h + 1) * head_dim]
    pl.semaphore_wait(barrier, 2 * n - 1)

    def team_copy(source, gathered, sems, origin, other):
        return remote(
            source,
            gathered.at[origin],
            sems.at[0, other],
            sems.at[1, origin],
            team * group_size + other,
            core,
        )

    def send_weights(k, carry):
        other = lax.rem(place + k, group_size)
        team_copy(paired_ref, paired_all, paired_sems, place, other).start()
        team_copy(down_ref, down_all, down_sems, place, other).start()
        return carry

    lax.fori_loop(1, group_size, send_weights, 0)
    paired_all[place] = paired_ref[...]
    down_all[place] = down_ref[...]

    block_len = min(256, cache_len)
    after_mask = (
        lax.broadcasted_iota(jnp.int32, (block_len, block_len), 0)
        > lax.broadcasted_iota(jnp.int32, (block_len, block_len), 1)
    ).astype(jnp.bfloat16)
    position = lax.broadcasted_iota(jnp.int32, (span * local_heads, block_len), 1)

    def attend(c, carry):
        keys_load(c).wait()
        lines = span * local_heads
        for i in range(span):
            s = c * span + i
            score_ref[s] = (
                jnp.dot(query_ref[s].astype(jnp.bfloat16), keys[s], preferred_element_type=f32)
                * head_dim ** (-0.5)
                + bias_ref[...]
            )
        limits = limits_ref[pl.ds(c * lines, lines)]
        later = jnp.zeros((lines, 1), f32)
        for first_pos in range(cache_len - block_len, -1, -block_len):
            columns = slice(first_pos, first_pos + block_len)
            scores = score_ref[pl.ds(c * span, span), :, columns].reshape(lines, block_len)
            visible = position + first_pos < limits
            keep = -(jnp.maximum(scores, 0.0) + jnp.log1p(jnp.exp(-jnp.abs(scores))))
            log_take = scores + keep
            keep = jnp.where(visible, keep, 0.0)
            top = keep.astype(jnp.bfloat16)
            rest = keep - top.astype(f32)
            middle = rest.astype(jnp.bfloat16)
            low = (rest - middle.astype(f32)).astype(jnp.bfloat16)
            sums = jnp.dot(
                jnp.concatenate([top, middle, low], axis=0),
                after_mask,
                preferred_element_type=f32,
            )
            after = sums[:lines] + sums[lines : 2 * lines] + sums[2 * lines :] + later
            later = later + jnp.sum(keep, axis=-1, keepdims=True)
            stick = jnp.where(visible, jnp.exp(log_take + after), 0.0)
            score_ref[pl.ds(c * span, span), :, columns] = stick.reshape(
                span, local_heads, block_len
            )
        values_load(c).wait()
        for i in range(span):
            s = c * span + i
            read_ref[s] = lax.dot_general(
                score_ref[s].astype(jnp.bfloat16),
                values[s],
                (((1,), (1,)), ((), ())),
                preferred_element_type=f32,
            )
        return carry

    lax.fori_loop(0, rows // span, attend, 0)
    heads_out = jnp.concatenate(
        [read_ref[:, h, :] for h in range(local_heads)], axis=1
    ).astype(jnp.bfloat16)
    loads[4].wait()
    attn_mine[...] = jnp.dot(heads_out, w_out[...], preferred_element_type=f32).astype(
        jnp.bfloat16
    )

    swap = remote(attn_mine, attn_peer, pair_sems.at[0], pair_sems.at[1], me, peer)
    swap.start()
    swap.wait()
    attn = attn_mine[...].astype(f32) + attn_peer[...].astype(f32)
    residual = (tokens_ref[...].astype(f32) + attn).astype(jnp.bfloat16)
    res_ref[...] = residual
    wide = residual.astype(f32)
    normed = (
        wide * lax.rsqrt(jnp.mean(wide * wide, axis=-1, keepdims=True) + 1e-06) * gain_ref[...]
    ).astype(jnp.bfloat16)
    norm_all[0, me] = normed[:, :half]
    norm_all[1, me] = normed[:, half:]

    def norm_copy(j, other):
        return remote(
            norm_all.at[core, j],
            norm_all.at[core, j],
            norm_sems.at[0, other],
            norm_sems.at[1, j],
            other,
            core,
        )

    def pass_copy(j, which):
        return remote(
            norm_all.at[which, j],
            norm_all.at[which, j],
            pass_sems.at[0, j],
            pass_sems.at[1, j],
            me,
            peer,
        )

    def send_norm(k, carry):
        norm_copy(me, lax.rem(me + k, n)).start()
        return carry

    lax.fori_loop(1, n, send_norm, 0)

    probs = jax.nn.sigmoid(jnp.dot(normed, router_ref[...], preferred_element_type=f32))
    expert_total = probs.shape[1]
    expert_index = lax.broadcasted_iota(jnp.int32, (rows, expert_total), 1)
    hits = jnp.zeros((rows, expert_total), f32)
    for k in range(routes_ref.shape[1]):
        hits = jnp.where(routes_ref[:, k : k + 1] == expert_index, 1.0, hits)
    picked = jnp.where(hits > 0.0, probs, 0.0)
    gates = picked / jnp.sum(picked, axis=-1, keepdims=True) * 2.5
    mix_gate = jax.nn.sigmoid(
        jnp.sum(normed.astype(f32) * mix_ref[...], axis=-1, keepdims=True)
    )

    for weight, target in ((w_key_ref, new_keys_ref), (w_value_ref, new_values_ref)):
        target[...] = jnp.dot(normed_ref[...], weight[...], preferred_element_type=f32).astype(
            jnp.bfloat16
        )

    def take_norm(k, carry):
        j = lax.rem(me + n - k, n)
        norm_copy(j, me).wait_recv()
        pass_copy(j, core).start()
        return carry

    lax.fori_loop(1, n, take_norm, 0)

    def take_pass(k, carry):
        pass_copy(lax.rem(me + n - k, n), peer).wait_recv()
        return carry

    lax.fori_loop(1, n, take_pass, 0)

    def part_copy(m, other):
        return remote(
            part_send.at[other],
            part_recv.at[m],
            part_sems.at[0, other],
            part_sems.at[1, m],
            other * group_size + place,
            core,
        )

    def back_copy(j, other):
        return remote(
            back_send.at[other],
            back_recv.at[j],
            back_sems.at[0, other],
            back_sems.at[1, j],
            other,
            core,
        )

    def dense_copy(m, other):
        return remote(
            dense_all.at[m],
            dense_all.at[m],
            dense_sems.at[0, other],
            dense_sems.at[1, m],
            other * group_size + place,
            core,
        )

    group = min(n, 16)
    groups = n // group
    block = group * rows

    def take_weights(k, carry):
        other = lax.rem(place + k, group_size)
        team_copy(paired_ref, paired_all, paired_sems, other, place).wait_recv()
        team_copy(down_ref, down_all, down_sems, other, place).wait_recv()
        return carry

    lax.fori_loop(1, group_size, take_weights, 0)
    features = jnp.concatenate(
        [norm_all[owner, m * group_size + place, :, pl.ds(lane, window)] for m in range(teams)],
        axis=0,
    )
    part_send[...] = (
        jnp.dot(
            features, paired_all[...].reshape(window, -1), preferred_element_type=f32
        )
        .astype(jnp.bfloat16)
        .reshape(part_send.shape)
    )

    def send_part(k, carry):
        part_copy(team, lax.rem(team + k, teams)).start()
        return carry

    lax.fori_loop(1, teams, send_part, 0)

    loads[1].wait()
    loads[2].wait()

    def expert_first(c, carry):
        base = c * group
        low = norm_all[0, pl.ds(base, group)].reshape(block, half)
        high = norm_all[1, pl.ds(base, group)].reshape(block, half)
        gate_rows = jnp.dot(low, w_gate[:half], preferred_element_type=f32) + jnp.dot(
            high, w_gate[half:], preferred_element_type=f32
        )
        up_rows = jnp.dot(low, w_up[:half], preferred_element_type=f32) + jnp.dot(
            high, w_up[half:], preferred_element_type=f32
        )
        hidden_ref[pl.ds(c, 1)] = (jax.nn.silu(gate_rows) * up_rows).astype(jnp.bfloat16)[None]
        return carry

    lax.fori_loop(0, groups, expert_first, 0)

    def take_part(k, total):
        m = lax.rem(team + teams - k, teams)
        part_copy(m, team).wait_recv()
        return total + part_recv[m].astype(f32)

    paired = lax.fori_loop(1, teams, take_part, part_send[team].astype(f32))
    hidden_cols = paired.shape[1] // 2
    dense_all[team] = (jax.nn.silu(paired[:, :hidden_cols]) * paired[:, hidden_cols:]).astype(
        jnp.bfloat16
    )

    def send_dense(k, carry):
        dense_copy(team, lax.rem(team + k, teams)).start()
        return carry

    lax.fori_loop(1, teams, send_dense, 0)

    loads[3].wait()
    far = pl.ds(pl.multiple_of(peer * half, half), half)
    near = pl.ds(pl.multiple_of(core * half, half), half)

    def expert_far(c, carry):
        value = jnp.dot(hidden_ref[c], w_down[:, far], preferred_element_type=f32)
        other_ref[pl.ds(c * group, group)] = value.astype(jnp.bfloat16).reshape(group, rows, half)
        return carry

    lax.fori_loop(0, groups, expert_far, 0)
    trade = remote(other_ref, peer_ref, pair_sems.at[2], pair_sems.at[3], me, peer)
    trade.start()

    def expert_near(c, carry):
        value = jnp.dot(hidden_ref[c], w_down[:, near], preferred_element_type=f32)
        mine_ref[pl.ds(c * group, group)] = value.astype(jnp.bfloat16).reshape(group, rows, half)
        return carry

    lax.fori_loop(0, groups, expert_near, 0)
    trade.wait()

    def send_back(k, carry):
        other = lax.rem(me + k, n)
        total = mine_ref[other].astype(f32) + peer_ref[other].astype(f32)
        back_send[other] = total.astype(jnp.bfloat16)

        @pl.when(k > 0)
        def _():
            back_copy(me, other).start()

        return carry

    lax.fori_loop(0, n, send_back, 0)

    def take_dense(k, carry):
        dense_copy(lax.rem(team + teams - k, teams), team).wait_recv()
        return carry

    lax.fori_loop(1, teams, take_dense, 0)
    cols_send[...] = (
        lax.dot_general(
            dense_all[...].reshape(teams * rows, hidden_cols),
            down_all[...].reshape(window, hidden_cols),
            (((1,), (1,)), ((), ())),
            preferred_element_type=f32,
        )
        .astype(jnp.bfloat16)
        .reshape(cols_send.shape)
    )

    def cols_copy(from_core, m, other, target):
        return remote(
            cols_send.at[other],
            cols_recv.at[from_core, m],
            cols_send_sem.at[other],
            cols_recv_sem.at[from_core, m],
            other * group_size + place,
            target,
        )

    def send_cols(k, carry):
        cols_copy(core, team, lax.rem(team + k, teams), owner).start()
        return carry

    lax.fori_loop(1, teams, send_cols, 0)

    @pl.when(owner == core)
    def _():
        cols_recv[core, team] = cols_send[team]

    @pl.when(owner != core)
    def _():
        cols_copy(core, team, team, peer).start()

    side = teams // 2

    def take_cols(k, carry):
        m = core * side + k

        @pl.when(m != team)
        def _():
            cols_copy(core, m, team, core).wait_recv()

        cols_copy(peer, m, team, core).wait_recv()
        return carry

    lax.fori_loop(0, side, take_cols, 0)
    dense = jnp.concatenate(
        [
            cols_recv[0, core * side + q].astype(f32) + cols_recv[1, core * side + q].astype(f32)
            for q in range(side)
        ],
        axis=1,
    )
    total = res_ref[:, near].astype(f32) + mix_gate * dense

    def take_back(k, total):
        j = lax.rem(me + n - k, n)

        @pl.when(k > 0)
        def _():
            back_copy(j, me).wait_recv()

        @pl.when(k == 0)
        def _():
            back_recv[me] = back_send[me]

        gate = jnp.sum(jnp.where(expert_index == j, gates, 0.0), axis=-1, keepdims=True)
        return total + gate * back_recv[j].astype(f32)

    out_ref[...] = lax.fori_loop(0, n, take_back, total).astype(jnp.bfloat16)

    def drain(k, carry):
        other = lax.rem(me + k, n)
        norm_copy(me, other).wait_send()
        pass_copy(other, core).wait_send()
        back_copy(me, other).wait_send()
        return carry

    lax.fori_loop(1, n, drain, 0)

    def drain_team(k, carry):
        other = lax.rem(place + k, group_size)
        team_copy(paired_ref, paired_all, paired_sems, place, other).wait_send()
        team_copy(down_ref, down_all, down_sems, place, other).wait_send()
        return carry

    lax.fori_loop(1, group_size, drain_team, 0)

    def drain_dense(k, carry):
        other = lax.rem(team + k, teams)
        part_copy(team, other).wait_send()
        dense_copy(team, other).wait_send()
        cols_copy(core, team, other, owner).wait_send()
        return carry

    lax.fori_loop(1, teams, drain_dense, 0)

    @pl.when(owner != core)
    def _():
        cols_copy(core, team, team, peer).wait_send()


def shards(
    n,
    tokens,
    lengths,
    attn_gain,
    w_query,
    w_key,
    w_value,
    head_bias,
    key_cache,
    value_cache,
    w_attn_out,
    ffn_gain,
    w_router,
    routes,
    w_dense_gate,
    w_dense_up,
    w_dense_down,
    dense_mix,
    w_expert_gate,
    w_expert_up,
    w_expert_down,
):
    rows, model = tokens.shape
    half = model // 2
    width, hidden_cols = w_dense_gate.shape
    group_size = min(n, max(4, 128 // width))
    teams = n // group_size
    window = width * group_size
    paired = jnp.concatenate([w_dense_gate, w_dense_up], axis=1)
    down = w_dense_down.T
    seq_count, local_kv, head_dim, cache_len = key_cache.shape
    local_heads = head_bias.shape[0]
    keys = key_cache.reshape(seq_count, head_dim, cache_len)
    values = value_cache.reshape(seq_count, head_dim, cache_len)
    limits = jnp.repeat(lengths, local_heads).reshape(seq_count * local_heads, 1)
    w_gate, w_up, w_down = w_expert_gate[0], w_expert_up[0], w_expert_down[0]
    expert_hidden = w_gate.shape[1]
    bf16, f32 = jnp.bfloat16, jnp.float32
    block = min(n, 16) * rows
    vmem = pl.BlockSpec(memory_space=pltpu.VMEM)
    anywhere = pl.BlockSpec(memory_space=pl.ANY)
    dma = pltpu.SemaphoreType.DMA
    return pl.pallas_call(
        functools.partial(whole_layer, n, group_size),
        out_shape=(
            jax.ShapeDtypeStruct((rows, half), bf16),
            jax.ShapeDtypeStruct((rows, w_key.shape[1]), bf16),
            jax.ShapeDtypeStruct((rows, w_value.shape[1]), bf16),
        ),
        in_specs=[vmem] * 12 + [anywhere] * 7,
        out_specs=(vmem, vmem, vmem),
        scratch_shapes=[
            pltpu.VMEM(w_query.shape, bf16),
            pltpu.VMEM(w_attn_out.shape, bf16),
            pltpu.VMEM(w_gate.shape, bf16),
            pltpu.VMEM(w_up.shape, bf16),
            pltpu.VMEM(w_down.shape, bf16),
            pltpu.VMEM(keys.shape, bf16),
            pltpu.VMEM(values.shape, bf16),
            dma((5,)),
            dma((rows // 4,)),
            dma((rows // 4,)),
            pltpu.VMEM((rows, local_heads, head_dim), f32),
            pltpu.VMEM((rows, local_heads, cache_len), f32),
            pltpu.VMEM((rows, local_heads, head_dim), f32),
            pltpu.VMEM((rows, model), bf16),
            pltpu.VMEM((group_size, width, 2 * hidden_cols), bf16),
            pltpu.VMEM((group_size, width, hidden_cols), bf16),
            pltpu.VMEM((rows, model), bf16),
            pltpu.VMEM((rows, model), bf16),
            pltpu.VMEM((rows, model), bf16),
            pltpu.VMEM((2, n, rows, half), bf16),
            pltpu.VMEM((teams, rows, 2 * hidden_cols), bf16),
            pltpu.VMEM((teams, rows, 2 * hidden_cols), bf16),
            pltpu.VMEM((n * rows // block, block, expert_hidden), bf16),
            pltpu.VMEM((teams, rows, hidden_cols), bf16),
            pltpu.VMEM((teams, rows, window), bf16),
            pltpu.VMEM((2, teams, rows, window), bf16),
            pltpu.VMEM((n, rows, half), bf16),
            pltpu.VMEM((n, rows, half), bf16),
            pltpu.VMEM((n, rows, half), bf16),
            pltpu.VMEM((n, rows, half), bf16),
            pltpu.VMEM((n, rows, half), bf16),
            dma((4,)),
            dma((2, group_size)),
            dma((2, group_size)),
            dma((2, n)),
            dma((2, n)),
            dma((2, teams)),
            dma((2, teams)),
            dma((teams,)),
            dma((2, teams)),
            dma((2, n)),
        ],
        compiler_params=pltpu.CompilerParams(
            collective_id=0, has_side_effects=True, vmem_limit_bytes=60 * 1024 * 1024
        ),
        name="whole_layer",
    )(
        tokens,
        attn_gain.reshape(1, model),
        limits,
        head_bias.reshape(local_heads, 1),
        w_key,
        w_value,
        ffn_gain.reshape(1, model),
        w_router,
        routes,
        dense_mix.reshape(1, model),
        paired,
        down,
        w_query,
        w_attn_out,
        w_gate,
        w_up,
        w_down,
        keys,
        values,
    )


def solution(mesh):
    return jax.shard_map(
        functools.partial(shards, mesh.shape["ep"]),
        mesh=mesh,
        in_specs=(
            P("ep", None),
            P("ep"),
            P(),
            P(None, "tp"),
            P(None, "tp"),
            P(None, "tp"),
            P("tp"),
            P("ep", "tp", None, None),
            P("ep", "tp", None, None),
            P("tp", None),
            P(),
            P(),
            P("ep", None),
            P("ep", "tp"),
            P("ep", "tp"),
            P("tp", "ep"),
            P(),
            P("ep", None, "tp"),
            P("ep", None, "tp"),
            P("ep", "tp", None),
        ),
        out_specs=(P("ep", "tp"), P("ep", "tp"), P("ep", "tp")),
        check_vma=False,
    )
```

time: 72.5 us -> 67.2 us (0.927)
  the two profiles are of different devices: /device:TPU:1 before, /device:TPU:7 now
where the time goes in v2:
time: 67.2 us; the launch traced here: 66.6 us
  Pallas kernels  49.9 us (74%)
  local copies, waits for them, and re-layouts  14.5 us (22%)
  other arithmetic  1.53 us (2%)
    pallas_call x1, Pallas kernels, shards(): pl.pallas_call(functools.partial(whole_layer, n, group_size), out_shape=(...  49.9 us
    unnamed x10, local copies, waits for them, and re-layouts  11.8 us
    concatenate x1, other arithmetic, shards(): paired = jnp.concatenate([w_dense_gate, w_dense_up], axis=1)  1.53 us
    reshape x1, local copies, waits for them, and re-layouts, shards(): head_bias.reshape(local_heads, 1)  1.35 us

profile of v2, /device:TPU:7, one launch (start us, length us, event | category | flops | bytes accessed | tf_op | source)
XLA Modules:
  0.0 66.6 jit_solution(9104311801167061478)
XLA Ops:
  0.6 0.0 copy-start
  0.6 1.4 %copy.32.bias_ref = f32[8,1]{1,0:T(8,128)} copy(f32[8,1]{0,1:T(1,128)} %bitcast.19) | data formatting | bytes 64 | tf_op jit(solution)/shard_map/reshape | solution.py:650
  2.0 0.7 %broadcast_in_dim.3 = s32[16,8]{1,0:T(8,128)S(1)} broadcast(s32[16]{0:T(128)} %param.21), dimensions={0} | broadcast | bytes 576 | tf_op jit(solution)/shard_map/broadcast_in_dim | solution.py:582
  2.7 1.4 %copy.36.routes_ref = s32[16,6]{1,0:T(8,128)} copy(s32[16,6]{0,1:T(8,128)} %param.32) | data formatting | bytes 768 | tf_op args[12]
  4.1 0.7 %reshape_reshape.4.limits_ref = s32[128,1]{1,0:T(8,128)} reshape(s32[16,8]{1,0:T(8,128)S(1)} %broadcast_in_dim.3) | data formatting | bytes 1024 | tf_op jit(solution)/shard_map/reshape;reshape | solution.py:582
  4.8 1.6 %copy.30 = bf16[256,128]{0,1:T(8,128)(2,1)} copy(bf16[256,128]{1,0:T(8,128)(2,1)} %param.35) | data formatting | bytes 131072 | tf_op args[15]
  6.3 1.5 %pad_maximum_fusion.paired_ref = bf16[128,512]{1,0:T(8,128)(2,1)} fusion(bf16[128,256]{1,0:T(8,128)(2,1)} %param.34, bf16[128,256]{1,0:T(8,128)(2,1)} %param.33), kind=kLoop, calls=%fused_computation | loop fusion | flops 262144 | bytes 262144 | tf_op jit(solution)/shard_map/concatenate | solution.py:576
  7.9 1.9 %copy.33.w_key_ref = bf16[2048,64]{1,0:T(8,128)(2,1)} copy(bf16[2048,64]{0,1:T(8,128)(2,1)} %param.24) | data formatting | bytes 524288 | tf_op args[4]
  9.8 1.9 %copy.34.w_value_ref = bf16[2048,64]{1,0:T(8,128)(2,1)} copy(bf16[2048,64]{0,1:T(8,128)(2,1)} %param.25) | data formatting | bytes 524288 | tf_op args[5]
  11.8 0.0 copy-done
  11.8 1.0 %copy.35.router_ref = bf16[2048,16]{1,0:T(8,128)(2,1)} copy(bf16[2048,16]{0,1:T(8,128)(2,1)S(1)} %copy-done) | data formatting | bytes 131072 | tf_op args[11]
  12.8 49.9 %whole_layer.1 = (bf16[16,1024]{1,0:T(8,128)(2,1)}, bf16[16,64]{1,0:T(8,128)(2,1)}, bf16[16,64]{1,0:T(8,128)(2,1)}) custom-call(bf16[16,2048]{1,0:T(8,128)(2,1)} %tokens_ref.1, f32[1,2048]{1,0:T(1,128)} %bitcast.16, s32[128,1]{1,0:T(8,128)} %reshape_reshape.4.limits_ref, f32[8,1]{1,0:T(8,128)} %copy.32.bias_ref, bf16[2048,64]{1,0:T(8,128)(2,1)} %copy.33.w_key_ref, ...), custom_call_target="tpu_custom_call" | custom-call | tf_op jit(solution)/shard_map/whole_layer/pallas_call | solution.py:590
  62.7 1.4 %copy.40 = bf16[16,1024]{1,0:T(8,128)(2,1)} copy(bf16[16,1024]{1,0:T(8,128)(2,1)} %get-tuple-element.6) | data formatting | bytes 65536
  64.1 1.3 %copy.41 = bf16[16,64]{1,0:T(8,128)(2,1)} copy(bf16[16,64]{1,0:T(8,128)(2,1)} %get-tuple-element.7) | data formatting | bytes 4096
  65.4 1.3 %copy.42 = bf16[16,64]{1,0:T(8,128)(2,1)} copy(bf16[16,64]{1,0:T(8,128)(2,1)} %get-tuple-element.8) | data formatting | bytes 4096
Async XLA Ops:
  0.6 11.1 %copy-start = (bf16[2048,16]{0,1:T(8,128)(2,1)S(1)}, bf16[2048,16]{0,1:T(8,128)(2,1)}, u32[]{:S(2)}) copy-start(bf16[2048,16]{0,1:T(8,128)(2,1)} %param.31) | copy-start | bytes 196612

commit v3 on v2

--- a/solution.py
+++ b/solution.py
@@ -15,7 +15,7 @@
     group_size,
     tokens_ref,
     attn_gain_ref,
-    limits_ref,
+    lengths_ref,
     bias_ref,
     w_key_ref,
     w_value_ref,
@@ -23,7 +23,8 @@
     router_ref,
     routes_ref,
     mix_ref,
-    paired_ref,
+    dense_gate_ref,
+    dense_up_ref,
     down_ref,
     w_query_hbm,
     w_out_hbm,
@@ -49,7 +50,8 @@
     score_ref,
     read_ref,
     normed_ref,
-    paired_all,
+    dense_gate_all,
+    dense_up_all,
     down_all,
     attn_mine,
     attn_peer,
@@ -67,7 +69,8 @@
     back_send,
     back_recv,
     pair_sems,
-    paired_sems,
+    dense_gate_sems,
+    dense_up_sems,
     down_sems,
     norm_sems,
     pass_sems,
@@ -82,7 +85,7 @@
     peer = 1 - core
     rows, model = tokens_ref.shape
     half = model // 2
-    width = paired_ref.shape[0]
+    width = dense_gate_ref.shape[0]
     window = width * group_size
     place = me % group_size
     team = me // group_size
@@ -91,7 +94,7 @@
     owner = first // half
     lane = pl.multiple_of(first % half, window)
     f32 = jnp.float32
-    local_heads = bias_ref.shape[0]
+    local_heads = bias_ref.shape[1]
     head_dim, cache_len = keys_hbm.shape[1:]
     span = 4
 
@@ -168,12 +171,14 @@
 
     def send_weights(k, carry):
         other = lax.rem(place + k, group_size)
-        team_copy(paired_ref, paired_all, paired_sems, place, other).start()
+        team_copy(dense_gate_ref, dense_gate_all, dense_gate_sems, place, other).start()
+        team_copy(dense_up_ref, dense_up_all, dense_up_sems, place, other).start()
         team_copy(down_ref, down_all, down_sems, place, other).start()
         return carry
 
     lax.fori_loop(1, group_size, send_weights, 0)
-    paired_all[place] = paired_ref[...]
+    dense_gate_all[place] = dense_gate_ref[...]
+    dense_up_all[place] = dense_up_ref[...]
     down_all[place] = down_ref[...]
 
     block_len = min(256, cache_len)
@@ -183,17 +188,26 @@
     ).astype(jnp.bfloat16)
     position = lax.broadcasted_iota(jnp.int32, (span * local_heads, block_len), 1)
 
+    head_row = lax.broadcasted_iota(jnp.int32, (local_heads, local_heads), 0)
+    head_col = lax.broadcasted_iota(jnp.int32, (local_heads, local_heads), 1)
+    bias = jnp.sum(jnp.where(head_row == head_col, bias_ref[...], 0.0), axis=1, keepdims=True)
+    lines = span * local_heads
+    line_seq = lax.broadcasted_iota(jnp.int32, (lines, rows), 0) // local_heads
+    seq_lane = lax.broadcasted_iota(jnp.int32, (lines, rows), 1)
+    lengths_row = lengths_ref[...].astype(f32)
+
     def attend(c, carry):
         keys_load(c).wait()
-        lines = span * local_heads
         for i in range(span):
             s = c * span + i
             score_ref[s] = (
                 jnp.dot(query_ref[s].astype(jnp.bfloat16), keys[s], preferred_element_type=f32)
                 * head_dim ** (-0.5)
-                + bias_ref[...]
+                + bias
             )
-        limits = limits_ref[pl.ds(c * lines, lines)]
+        limits = jnp.sum(
+            jnp.where(seq_lane == line_seq + c * span, lengths_row, 0.0), axis=1, keepdims=True
+        ).astype(jnp.int32)
         later = jnp.zeros((lines, 1), f32)
         for first_pos in range(cache_len - block_len, -1, -block_len):
             columns = slice(first_pos, first_pos + block_len)
@@ -276,22 +290,26 @@
 
     lax.fori_loop(1, n, send_norm, 0)
 
-    probs = jax.nn.sigmoid(jnp.dot(normed, router_ref[...], preferred_element_type=f32))
-    expert_total = probs.shape[1]
+    across = (((1,), (1,)), ((), ()))
+    probs = jax.nn.sigmoid(
+        lax.dot_general(router_ref[...], normed, across, preferred_element_type=f32)
+    )
+    expert_total = probs.shape[0]
+    expert_row = lax.broadcasted_iota(jnp.int32, (expert_total, rows), 0)
+    hits = jnp.zeros((expert_total, rows), f32)
+    for k in range(routes_ref.shape[0]):
+        hits = jnp.where(routes_ref[k : k + 1, :] == expert_row, 1.0, hits)
+    picked = jnp.where(hits > 0.0, probs, 0.0)
+    gates = (picked / jnp.sum(picked, axis=0, keepdims=True) * 2.5).T
     expert_index = lax.broadcasted_iota(jnp.int32, (rows, expert_total), 1)
-    hits = jnp.zeros((rows, expert_total), f32)
-    for k in range(routes_ref.shape[1]):
-        hits = jnp.where(routes_ref[:, k : k + 1] == expert_index, 1.0, hits)
-    picked = jnp.where(hits > 0.0, probs, 0.0)
-    gates = picked / jnp.sum(picked, axis=-1, keepdims=True) * 2.5
     mix_gate = jax.nn.sigmoid(
         jnp.sum(normed.astype(f32) * mix_ref[...], axis=-1, keepdims=True)
     )
 
     for weight, target in ((w_key_ref, new_keys_ref), (w_value_ref, new_values_ref)):
-        target[...] = jnp.dot(normed_ref[...], weight[...], preferred_element_type=f32).astype(
-            jnp.bfloat16
-        )
+        target[...] = lax.dot_general(
+            normed_ref[...], weight[...], across, preferred_element_type=f32
+        ).astype(jnp.bfloat16)
 
     def take_norm(k, carry):
         j = lax.rem(me + n - k, n)
@@ -343,7 +361,8 @@
 
     def take_weights(k, carry):
         other = lax.rem(place + k, group_size)
-        team_copy(paired_ref, paired_all, paired_sems, other, place).wait_recv()
+        team_copy(dense_gate_ref, dense_gate_all, dense_gate_sems, other, place).wait_recv()
+        team_copy(dense_up_ref, dense_up_all, dense_up_sems, other, place).wait_recv()
         team_copy(down_ref, down_all, down_sems, other, place).wait_recv()
         return carry
 
@@ -352,13 +371,15 @@
         [norm_all[owner, m * group_size + place, :, pl.ds(lane, window)] for m in range(teams)],
         axis=0,
     )
-    part_send[...] = (
-        jnp.dot(
-            features, paired_all[...].reshape(window, -1), preferred_element_type=f32
-        )
-        .astype(jnp.bfloat16)
-        .reshape(part_send.shape)
-    )
+    hidden_cols = dense_gate_ref.shape[1]
+    for gathered, columns in (
+        (dense_gate_all, slice(0, hidden_cols)),
+        (dense_up_all, slice(hidden_cols, 2 * hidden_cols)),
+    ):
+        value = jnp.dot(
+            features, gathered[...].reshape(window, hidden_cols), preferred_element_type=f32
+        )
+        part_send[:, :, columns] = value.astype(jnp.bfloat16).reshape(teams, rows, hidden_cols)
 
     def send_part(k, carry):
         part_copy(team, lax.rem(team + k, teams)).start()
@@ -390,7 +411,6 @@
         return total + part_recv[m].astype(f32)
 
     paired = lax.fori_loop(1, teams, take_part, part_send[team].astype(f32))
-    hidden_cols = paired.shape[1] // 2
     dense_all[team] = (jax.nn.silu(paired[:, :hidden_cols]) * paired[:, hidden_cols:]).astype(
         jnp.bfloat16
     )
@@ -440,15 +460,12 @@
         return carry
 
     lax.fori_loop(1, teams, take_dense, 0)
+    dense_rows = dense_all[...].reshape(teams * rows, hidden_cols)
+    columns = [
+        jnp.dot(dense_rows, down_all[q], preferred_element_type=f32) for q in range(group_size)
+    ]
     cols_send[...] = (
-        lax.dot_general(
-            dense_all[...].reshape(teams * rows, hidden_cols),
-            down_all[...].reshape(window, hidden_cols),
-            (((1,), (1,)), ((), ())),
-            preferred_element_type=f32,
-        )
-        .astype(jnp.bfloat16)
-        .reshape(cols_send.shape)
+        jnp.concatenate(columns, axis=1).astype(jnp.bfloat16).reshape(cols_send.shape)
     )
 
     def cols_copy(from_core, m, other, target):
@@ -524,7 +541,8 @@
 
     def drain_team(k, carry):
         other = lax.rem(place + k, group_size)
-        team_copy(paired_ref, paired_all, paired_sems, place, other).wait_send()
+        team_copy(dense_gate_ref, dense_gate_all, dense_gate_sems, place, other).wait_send()
+        team_copy(dense_up_ref, dense_up_all, dense_up_sems, place, other).wait_send()
         team_copy(down_ref, down_all, down_sems, place, other).wait_send()
         return carry
 
@@ -573,19 +591,16 @@
     group_size = min(n, max(4, 128 // width))
     teams = n // group_size
     window = width * group_size
-    paired = jnp.concatenate([w_dense_gate, w_dense_up], axis=1)
-    down = w_dense_down.T
     seq_count, local_kv, head_dim, cache_len = key_cache.shape
     local_heads = head_bias.shape[0]
     keys = key_cache.reshape(seq_count, head_dim, cache_len)
     values = value_cache.reshape(seq_count, head_dim, cache_len)
-    limits = jnp.repeat(lengths, local_heads).reshape(seq_count * local_heads, 1)
     w_gate, w_up, w_down = w_expert_gate[0], w_expert_up[0], w_expert_down[0]
     expert_hidden = w_gate.shape[1]
     bf16, f32 = jnp.bfloat16, jnp.float32
     block = min(n, 16) * rows
     vmem = pl.BlockSpec(memory_space=pltpu.VMEM)
-    anywhere = pl.BlockSpec(memory_space=pl.ANY)
+    anywhere = pl.BlockSpec(memory_space=pltpu.HBM)
     dma = pltpu.SemaphoreType.DMA
     return pl.pallas_call(
         functools.partial(whole_layer, n, group_size),
@@ -594,7 +609,7 @@
             jax.ShapeDtypeStruct((rows, w_key.shape[1]), bf16),
             jax.ShapeDtypeStruct((rows, w_value.shape[1]), bf16),
         ),
-        in_specs=[vmem] * 12 + [anywhere] * 7,
+        in_specs=[vmem] * 13 + [anywhere] * 7,
         out_specs=(vmem, vmem, vmem),
         scratch_shapes=[
             pltpu.VMEM(w_query.shape, bf16),
@@ -611,8 +626,9 @@
             pltpu.VMEM((rows, local_heads, cache_len), f32),
             pltpu.VMEM((rows, local_heads, head_dim), f32),
             pltpu.VMEM((rows, model), bf16),
-            pltpu.VMEM((group_size, width, 2 * hidden_cols), bf16),
             pltpu.VMEM((group_size, width, hidden_cols), bf16),
+            pltpu.VMEM((group_size, width, hidden_cols), bf16),
+            pltpu.VMEM((group_size, hidden_cols, width), bf16),
             pltpu.VMEM((rows, model), bf16),
             pltpu.VMEM((rows, model), bf16),
             pltpu.VMEM((rows, model), bf16),
@@ -631,6 +647,7 @@
             dma((4,)),
             dma((2, group_size)),
             dma((2, group_size)),
+            dma((2, group_size)),
             dma((2, n)),
             dma((2, n)),
             dma((2, teams)),
@@ -640,22 +657,23 @@
             dma((2, n)),
         ],
         compiler_params=pltpu.CompilerParams(
-            collective_id=0, has_side_effects=True, vmem_limit_bytes=60 * 1024 * 1024
+            collective_id=0, has_side_effects=True, vmem_limit_bytes=63 * 1024 * 1024
         ),
         name="whole_layer",
     )(
         tokens,
         attn_gain.reshape(1, model),
-        limits,
-        head_bias.reshape(local_heads, 1),
-        w_key,
-        w_value,
+        lengths.reshape(1, seq_count),
+        head_bias.reshape(1, local_heads),
+        w_key.T,
+        w_value.T,
         ffn_gain.reshape(1, model),
-        w_router,
-        routes,
+        w_router.T,
+        routes.T,
         dense_mix.reshape(1, model),
-        paired,
-        down,
+        w_dense_gate,
+        w_dense_up,
+        w_dense_down,
         w_query,
         w_attn_out,
         w_gate,

time: 67.2 us -> 54.6 us (0.81)
  local copies, waits for them, and re-layouts: 14.5 us -> 3.91 us
  other arithmetic: 1.53 us -> 0 us
    unnamed x10 -> x3, local copies, waits for them, and re-layouts: 11.8 us -> 3.91 us
    concatenate x1 -> x0, other arithmetic: 1.53 us -> none  [shards(): paired = jnp.concatenate([w_dense_gate, w_dense_up], axis=1)]
    reshape x1 -> x0, local copies, waits for them, and re-layouts: 1.35 us -> none  [shards(): head_bias.reshape(local_heads, 1)]
    broadcast_in_dim x1 -> x0, local copies, waits for them, and re-layouts: 0.72 us -> none  [shards(): jnp.repeat(lengths, local_heads).reshape(seq_count * local_heads, 1)]
    another operation x1 -> x0, local copies, waits for them, and re-layouts: 0.7 us -> none  [shards(): jnp.repeat(lengths, local_heads).reshape(seq_count * local_heads, 1)]
where the time goes in v3:
time: 54.6 us; the launch traced here: 54.3 us
  Pallas kernels  49.8 us (91%)
  local copies, waits for them, and re-layouts  3.91 us (7%)
  between operations  0.65 us (1%)
    pallas_call x1, Pallas kernels, shards(): pl.pallas_call(functools.partial(whole_layer, n, group_size), out_shape=(...  49.8 us
    unnamed x3, local copies, waits for them, and re-layouts  3.91 us

profile of v3, /device:TPU:7, one launch (start us, length us, event | category | flops | bytes accessed | tf_op | source)
XLA Modules:
  0.0 54.3 jit_solution(3005432509352608028)
XLA Ops:
  0.6 49.8 %whole_layer.1 = (bf16[16,1024]{1,0:T(8,128)(2,1)}, bf16[16,64]{1,0:T(8,128)(2,1)}, bf16[16,64]{1,0:T(8,128)(2,1)}) custom-call(bf16[16,2048]{1,0:T(8,128)(2,1)} %tokens_ref.1, f32[1,2048]{1,0:T(1,128)} %bitcast.22, s32[1,16]{1,0:T(1,128)} %bitcast.26, f32[1,8]{1,0:T(1,128)} %bitcast.27, bf16[64,2048]{1,0:T(8,128)(2,1)} %bitcast.19, ...), custom_call_target="tpu_custom_call" | custom-call | tf_op jit(solution)/shard_map/whole_layer/pallas_call | solution.py:605
  50.4 1.4 %copy.26 = bf16[16,1024]{1,0:T(8,128)(2,1)} copy(bf16[16,1024]{1,0:T(8,128)(2,1)} %get-tuple-element.6) | data formatting | bytes 65536
  51.8 1.3 %copy.27 = bf16[16,64]{1,0:T(8,128)(2,1)} copy(bf16[16,64]{1,0:T(8,128)(2,1)} %get-tuple-element.7) | data formatting | bytes 4096
  53.1 1.3 %copy.28 = bf16[16,64]{1,0:T(8,128)(2,1)} copy(bf16[16,64]{1,0:T(8,128)(2,1)} %get-tuple-element.8) | data formatting | bytes 4096
